TPU v7x, 32 devices: a whole 2x2x4 slice. The times are simulated.
32 devices in a mesh: sp: 4 (over z), fs: 4 (over y, x), tp: 2 (over core).
Axes of the slice: x: 2, y: 2, z: 4, core: 2. Of those that a mesh axis runs over, the one named last changes fastest.
Arguments:
- tokens: bfloat16 [4, 1024, 2048], P('fs', 'sp', 'tp'), may hold values from -6 to 6
- norm_gain: float32 [2048], replicated, may hold values from 0.1 to 1.9
- memory_query: bfloat16 [2048, 1024], P('fs', 'tp'), may hold values from -0.125 to 0.125
- memory_key: bfloat16 [2048, 1024], P('fs', 'tp'), may hold values from -0.125 to 0.125
- memory_value: bfloat16 [2048, 1024], P('fs', 'tp'), may hold values from -0.125 to 0.125
- memory_outgate: bfloat16 [2048, 1024], P('fs', 'tp'), may hold values from -0.125 to 0.125
- memory_ingate: bfloat16 [2048, 4], P(None, 'tp'), may hold values from -0.125 to 0.125
- memory_forget: bfloat16 [2048, 4], P(None, 'tp'), may hold values from -0.125 to 0.125
- forget_bias: float32 [4], P('tp'), may hold values from 3 to 13
- forget_shift: float32 [4, 1024, 4], P('fs', 'sp', 'tp'), may hold values from -1.6 to 0
- stick_query: bfloat16 [2048, 512], P(None, 'tp'), may hold values from -0.125 to 0.125
- stick_key: bfloat16 [2048, 512], P(None, 'tp'), may hold values from -0.125 to 0.125
- stick_value: bfloat16 [2048, 512], P(None, 'tp'), may hold values from -0.125 to 0.125
- stick_bias: float32 [4], P('tp'), may hold values from -11 to -2
- memory_gain: float32 [1024], P('tp'), may hold values from 0.1 to 1.9
- stick_gain: float32 [512], P('tp'), may hold values from 0.1 to 1.9
- out_memory: bfloat16 [1024, 2048], P('tp'), may hold values from -0.15625 to 0.15625
- out_stick: bfloat16 [512, 2048], P('tp'), may hold values from -0.15625 to 0.15625
Outputs:
- mixed: bfloat16 [4, 1024, 2048], P('fs', ('sp', 'tp'))
All inputs are finite; a program needn't handle non-finite values.
Results may differ from a plain program's by a relative error of at most 0.015.
Values may be sent and summed in bfloat16 or wider, within the bound.
A program may use at most 128 MiB of HBM per device.

v0:
```python
import functools

import jax
import jax.numpy as jnp
from jax import lax
from jax.experimental import pallas as pl
from jax.experimental.pallas import tpu as pltpu
from jax.sharding import PartitionSpec as P

MESH = pl.DeviceIdType.MESH
epsilon = 1e-06
floor_neg = -1e30
f32 = jnp.float32
bf16 = jnp.bfloat16

KEY, VALUE, QUERY, GATE = 0, 1, 2, 3


def dot(a, b, dims=((1,), (0,))):
    return lax.dot_general(a, b, (dims, ((), ())), preferred_element_type=f32)


def softplus(z):
    return jnp.maximum(z, 0.0) + jnp.log(1.0 + jnp.exp(-jnp.abs(z)))


def kernel(
    n_sp,
    n_out,
    tok_ref,
    gain_ref,
    ingate_ref,
    forget_ref,
    bias_ref,
    shift_ref,
    sbias_ref,
    mgain_ref,
    sgain_ref,
    wk_hbm,
    wv_hbm,
    wq_hbm,
    wo_hbm,
    sq_hbm,
    sk_hbm,
    sv_hbm,
    om_hbm,
    os_hbm,
    out_ref,
    tok_in,
    nrm,
    xg,
    wm,
    wg,
    ws,
    wout,
    sb,
    rb,
    own_part,
    proj,
    squery,
    kv,
    stick_acc,
    stick_run,
    gw,
    u_rows,
    u_cols,
    totals,
    tops,
    state_own,
    state_in,
    state_out,
    log_in,
    log_out,
    mix,
    ob,
    orb,
    load_sem,
    tok_s,
    tok_r,
    a2a_s,
    a2a_r,
    fwd_s,
    fwd_r,
    w_s,
    w_r,
    rs_s,
    rs_r,
    kv_s,
    kv_r,
    chain_s,
    chain_r,
    log_s,
    log_r,
    out_s,
    out_r,
):
    f = lax.axis_index("fs")
    s = lax.axis_index("sp")
    t = lax.axis_index("tp")
    rows, half_feat = tok_ref.shape
    heads = state_own.shape[0]
    dm = state_own.shape[1]
    ds = sgain_ref.shape[1] // heads
    block = wm.shape[1]
    half = rows // 2
    other = 1 - t

    def flip(bits):
        if bits == 3:
            return 3 - f
        if bits == 1:
            return f + 1 - 2 * (f % 2)
        return f + 2 - 4 * (f // 2)

    def remote(src, dst, send, recv, device):
        return pltpu.make_async_remote_copy(
            src_ref=src,
            dst_ref=dst,
            send_sem=send,
            recv_sem=recv,
            device_id=device,
            device_id_type=MESH,
        )

    barrier = pltpu.get_barrier_semaphore()
    pl.semaphore_signal(barrier, inc=1, device_id={"tp": other}, device_id_type=MESH)
    for bits in (1, 2, 3):
        pl.semaphore_signal(barrier, inc=1, device_id={"fs": flip(bits)}, device_id_type=MESH)

    @pl.when(s > 0)
    def _():
        pl.semaphore_signal(barrier, inc=1, device_id={"sp": s - 1}, device_id_type=MESH)

    @pl.when(s < n_sp - 1)
    def _():
        pl.semaphore_signal(barrier, inc=1, device_id={"sp": s + 1}, device_id_type=MESH)

    width_s = ws.shape[2]
    loads = [
        pltpu.make_async_copy(sq_hbm, ws.at[0], load_sem.at[0]),
        pltpu.make_async_copy(sk_hbm, ws.at[1], load_sem.at[1]),
        pltpu.make_async_copy(sv_hbm, ws.at[2], load_sem.at[2]),
        pltpu.make_async_copy(wk_hbm, wm.at[0], load_sem.at[3]),
        pltpu.make_async_copy(wv_hbm, wm.at[1], load_sem.at[4]),
        pltpu.make_async_copy(wq_hbm, wm.at[2], load_sem.at[5]),
        pltpu.make_async_copy(wo_hbm, wm.at[3], load_sem.at[6]),
        pltpu.make_async_copy(om_hbm, wout.at[pl.ds(0, heads * dm)], load_sem.at[7]),
        pltpu.make_async_copy(os_hbm, wout.at[pl.ds(heads * dm, heads * ds)], load_sem.at[8]),
    ]
    for at in (3, 4, 0, 1, 2, 5, 6, 7, 8):
        loads[at].start()

    peers = 4 + jnp.where(s > 0, 1, 0) + jnp.where(s < n_sp - 1, 1, 0)
    pl.semaphore_wait(barrier, peers)

    tok_copy = remote(tok_ref, tok_in, tok_s.at[0], tok_r.at[0], {"tp": other})
    tok_copy.start()

    def pair_bits(h):
        return 1 if h % 2 == 0 else 2

    def sum_bits(h):
        return 3 - pair_bits(h)

    def weight_copy(p, h):
        at = p * heads + h
        return remote(
            wm.at[p, :, pl.ds(h * dm, dm)], wg.at[p, h], w_s.at[at], w_r.at[at],
            {"fs": flip(pair_bits(h))},
        )

    def send_weight(p):
        loads[3 + p].wait()
        for h in range(heads):
            weight_copy(p, h).start()

    send_weight(KEY)
    tok_copy.wait_recv()

    step_rows = 32
    own_cols = pl.ds(pl.multiple_of(t * half_feat, half_feat), half_feat)
    far_cols = pl.ds(pl.multiple_of(other * half_feat, half_feat), half_feat)

    def norm_rows(i, _):
        at = pl.ds(pl.multiple_of(i * step_rows, step_rows), step_rows)
        own = tok_ref[at, :].astype(f32)
        far = tok_in[at, :].astype(f32)
        total = jnp.sum(own * own, axis=1, keepdims=True) + jnp.sum(far * far, axis=1, keepdims=True)
        scale = lax.rsqrt(total / (2 * half_feat) + epsilon)
        nrm[at, own_cols] = (own * scale * gain_ref[:, own_cols]).astype(bf16)
        nrm[at, far_cols] = (far * scale * gain_ref[:, far_cols]).astype(bf16)
        return 0

    lax.fori_loop(0, rows // step_rows, norm_rows, 0)

    my_rows = pl.ds(pl.multiple_of(t * half, half), half)

    def feature_block(index):
        return pl.ds(pl.multiple_of(index * block, block), block)

    a2a, fwd = {}, {}
    for h in range(heads):
        for which in range(2):
            at = h * 2 + which
            to = flip(sum_bits(h))
            a2a[at] = remote(
                nrm.at[my_rows, feature_block(to if which == 0 else flip(3))],
                xg.at[h, which, my_rows],
                a2a_s.at[at],
                a2a_r.at[at],
                {"fs": to},
            )
            a2a[at].start()
    send_weight(VALUE)

    for load in loads[:3]:
        load.wait()
    normed = nrm[...]
    kv[0, 0] = dot(normed, ws[1]).astype(bf16)
    kv[0, 1] = dot(normed, ws[2]).astype(bf16)

    def kv_copy(d):
        return remote(kv.at[d - 1], kv.at[d], kv_s.at[d], kv_r.at[d], {"sp": s + 1})

    def kv_send(d):
        @pl.when((s < n_sp - 1) & (s >= d - 1))
        def _():
            kv_copy(d).start()

    kv_send(1)
    squery[...] = dot(normed, ws[0]).astype(bf16)

    row_at = lax.broadcasted_iota(jnp.int32, (rows, rows), 0)
    col_at = lax.broadcasted_iota(jnp.int32, (rows, rows), 1)
    gw[...] = jnp.zeros(gw.shape, bf16)
    gw[0:heads, :] = ingate_ref[...]
    gw[8 : 8 + heads, :] = forget_ref[...]
    gate = dot(gw[...], normed, ((1,), (1,)))
    triu = (row_at <= col_at).astype(f32)
    u_rows[...] = jnp.zeros(u_rows.shape, f32)
    for h in range(heads):
        log_forget = shift_ref[h : h + 1, :] - softplus(-(gate[8 + h : 9 + h, :] + bias_ref[h]))
        cumulative = lax.dot_general(
            jnp.broadcast_to(log_forget, (8, rows)), triu, (((1,), (0,)), ((), ())),
            precision=lax.Precision.HIGHEST, preferred_element_type=f32,
        )
        u_rows[h : h + 1, :] = gate[h : h + 1, :] - cumulative[0:1, :]
        totals[h : h + 1, :] = jnp.broadcast_to(
            cumulative[0:1, rows - 1 : rows], (1, totals.shape[1])
        )
    u_cols[...] = jnp.transpose(u_rows[...])

    def stick_part(h, kv_at, diagonal):
        cols = slice(h * ds, (h + 1) * ds)
        z = dot(squery[:, cols], kv[kv_at, 0, :, cols], ((1,), (1,)))
        z = z * ds ** (-0.5) + sbias_ref[h]
        keep = -softplus(z)
        visible = col_at < row_at
        if diagonal:
            kept = jnp.where(visible, keep, 0.0)
        else:
            kept = keep
        strict = (row_at > col_at).astype(bf16)
        high = kept.astype(bf16)
        low = (kept - high.astype(f32)).astype(bf16)
        after = dot(high, strict) + dot(low, strict)
        weights = jnp.exp(z + keep + after)
        if diagonal:
            weights = jnp.where(visible, weights, 0.0)
        part = dot(weights.astype(bf16), kv[kv_at, 1, :, cols])
        return part, jnp.sum(kept, axis=1, keepdims=True)

    def stick_own():
        for h in range(heads):
            part, keep = stick_part(h, 0, True)
            stick_acc[h] = part
            stick_run[h] = jnp.broadcast_to(keep, stick_run.shape[1:])

    def stick_span(d):
        @pl.when(s >= d)
        def _():
            remote(kv.at[d - 1], kv.at[d], kv_s.at[d], kv_r.at[d], {"sp": s - 1}).wait_recv()

        kv_next(d)

        @pl.when(s >= d)
        def _():
            for h in range(heads):
                part, keep = stick_part(h, d, False)
                stick_acc[h] = stick_acc[h] + jnp.exp(stick_run[h]) * part
                stick_run[h] = stick_run[h] + keep

    def kv_next(d):
        @pl.when((s < n_sp - 1) & (s >= d) & (d < n_sp - 1))
        def _():
            kv_copy(d + 1).start()

    def stick_spans(low, high):
        if high > low:
            lax.fori_loop(low, high, lambda d, c: (stick_span(d), c)[1], 0)

    stick_own()
    for at in range(2 * heads):
        a2a[at].wait_recv()
        h, which = divmod(at, 2)
        fwd[at] = remote(
            xg.at[h, which, my_rows],
            xg.at[h, which, my_rows],
            fwd_s.at[at],
            fwd_r.at[at],
            {"tp": other},
        )
        fwd[at].start()

    def rs_copy(p, h):
        at = p * heads + h
        return remote(
            sb.at[p, h], rb.at[p, h], rs_s.at[at], rs_r.at[at], {"fs": flip(sum_bits(h))}
        )

    def partials(p):
        for h in range(heads):
            cols = slice(h * dm, (h + 1) * dm)
            if p == KEY:
                fwd[2 * h].wait_recv()
                fwd[2 * h + 1].wait_recv()
            weight_copy(p, h).wait_recv()
            sb[p, h] = (dot(xg[h, 0], wm[p, :, cols]) + dot(xg[h, 1], wg[p, h])).astype(bf16)
            rs_copy(p, h).start()

    def own_partials(p):
        for h in range(heads):
            cols = slice(h * dm, (h + 1) * dm)
            own_part[p, h] = dot(nrm[:, feature_block(f)], wm[p, :, cols]) + dot(
                nrm[:, feature_block(flip(pair_bits(h)))], wg[p, h]
            )

    def finish(p, h):
        rs_copy(p, h).wait_recv()
        return (own_part[p, h] + rb[p, h].astype(f32)).astype(bf16)

    partials(KEY)
    own_partials(KEY)
    partials(VALUE)
    send_weight(QUERY)
    send_weight(GATE)
    own_partials(VALUE)
    stick_spans(1, min(2, n_sp))

    def column(h):
        return u_cols[:, h : h + 1]

    for h in range(heads):
        proj[KEY, h] = (finish(KEY, h).astype(f32) * dm ** (-0.5)).astype(bf16)
        proj[VALUE, h] = finish(VALUE, h)
        u = column(h)
        top = jnp.max(u, axis=0, keepdims=True)
        weighted = (proj[KEY, h].astype(f32) * jnp.exp(u - top)).astype(bf16)
        state_own[h] = dot(weighted, proj[VALUE, h], ((0,), (0,)))

    def log_copy(to):
        return remote(log_out, log_in, log_s.at[0], log_r.at[0], {"sp": to})

    piece_dm = dm // 2
    pieces = 4

    def chain_copy(h, c, to):
        lines = pl.ds(c // 2 * piece_dm, piece_dm)
        cols = pl.ds(c % 2 * piece_dm, piece_dm)
        at = h * pieces + c
        return remote(
            state_out.at[h, lines, cols], state_in.at[h, lines, cols], chain_s.at[at], chain_r.at[at],
            {"sp": to},
        )

    def chain():
        @pl.when(s == 0)
        def _():
            log_in[...] = jnp.full(log_in.shape, floor_neg, f32)
            state_in[...] = jnp.zeros(state_in.shape, bf16)

        @pl.when(s > 0)
        def _():
            log_copy(s - 1).wait_recv()

        factors = []
        for h in range(heads):
            total = totals[h : h + 1, 0:1]
            early = total + log_in[h : h + 1, 0:1]
            late = total + jnp.max(column(h), axis=0, keepdims=True)
            top = jnp.maximum(early, late)
            log_out[h : h + 1, :] = jnp.broadcast_to(top, (1, log_out.shape[1]))
            factors.append((jnp.exp(early - top), jnp.exp(late - top)))

        @pl.when(s < n_sp - 1)
        def _():
            log_copy(s + 1).start()

        for at in range(pieces * heads):
            h, c = divmod(at, pieces)
            lines = pl.ds(c // 2 * piece_dm, piece_dm)
            cols = pl.ds(c % 2 * piece_dm, piece_dm)

            @pl.when(s > 0)
            def _():
                chain_copy(h, c, s - 1).wait_recv()

            @pl.when(s < n_sp - 1)
            def _():
                early, late = factors[h]
                state_out[h, lines, cols] = (
                    early * state_in[h, lines, cols].astype(f32) + late * state_own[h, lines, cols]
                ).astype(bf16)
                chain_copy(h, c, s + 1).start()

    log_out[...] = jnp.zeros(log_out.shape, f32)
    pl.when(s == 0)(chain)
    stick_spans(2, min(3, n_sp))
    partials(QUERY)
    pl.when(s == 1)(chain)
    own_partials(QUERY)
    pl.when(s == 2)(chain)
    partials(GATE)
    own_partials(GATE)
    stick_spans(3, n_sp)
    for load in loads[7:]:
        load.wait()

    for h in range(heads):
        cols = slice(h * ds, (h + 1) * ds)
        out = stick_acc[h]
        scale = lax.rsqrt(jnp.mean(out * out, axis=1, keepdims=True) + epsilon)
        mix[:, heads * dm + h * ds : heads * dm + (h + 1) * ds] = (
            out * scale * sgain_ref[:, cols]
        ).astype(bf16)

    causal = col_at <= row_at
    for h in range(heads):
        proj[QUERY, h] = finish(QUERY, h)
        masked = jnp.where(causal, u_rows[h : h + 1, :], floor_neg)
        top = jnp.max(masked, axis=1, keepdims=True)
        scores = dot(proj[QUERY, h], proj[KEY, h], ((1,), (1,))) * jnp.exp(masked - top)
        own_part[QUERY, h] = dot(scores.astype(bf16), proj[VALUE, h])
        tops[h] = jnp.broadcast_to(top, tops.shape[1:])
    pl.when(s > 2)(chain)
    for h in range(heads):
        carried_max = log_in[h : h + 1, 0:1]
        top = tops[h, :, 0:1]
        running = jnp.maximum(carried_max, top)
        own_part[QUERY, h] = jnp.exp(top - running) * own_part[QUERY, h] + jnp.exp(
            carried_max - running
        ) * dot(proj[QUERY, h], state_in[h])
    for h in range(heads):
        gated = own_part[QUERY, h] / (1.0 + jnp.exp(-finish(GATE, h).astype(f32)))
        scale = lax.rsqrt(jnp.mean(gated * gated, axis=1, keepdims=True) + epsilon)
        cols = slice(h * dm, (h + 1) * dm)
        mix[:, cols] = (gated * scale * mgain_ref[:, cols]).astype(bf16)

    piece = wout.shape[1] // n_out
    far_rows = pl.ds(pl.multiple_of(other * half, half), half)
    copies = []
    for c in range(n_out):
        cols = slice(c * piece, (c + 1) * piece)
        ob[c] = dot(mix[far_rows, :], wout[:, cols]).astype(bf16)
        copy = remote(ob.at[c], orb.at[c], out_s.at[c], out_r.at[c], {"tp": other})
        copy.start()
        copies.append(copy)
    for c in range(n_out):
        cols = slice(c * piece, (c + 1) * piece)
        mine = dot(mix[my_rows, :], wout[:, cols])
        copies[c].wait_recv()
        out_ref[:, cols] = (mine + orb[c].astype(f32)).astype(bf16)

    tok_copy.wait_send()
    for at in range(2 * heads):
        a2a[at].wait_send()
        fwd[at].wait_send()
    for p in range(4):
        for h in range(heads):
            weight_copy(p, h).wait_send()
            rs_copy(p, h).wait_send()
    for copy in copies:
        copy.wait_send()

    @pl.when(s < n_sp - 1)
    def _():
        log_copy(s + 1).wait_send()
        for at in range(pieces * heads):
            chain_copy(at // pieces, at % pieces, s + 1).wait_send()

    def kv_done(d, c):
        @pl.when((s < n_sp - 1) & (s >= d - 1))
        def _():
            kv_copy(d).wait_send()

        return c

    if n_sp > 1:
        lax.fori_loop(1, n_sp, kv_done, 0)


def per_device(
    n_sp,
    tokens,
    norm_gain,
    memory_query,
    memory_key,
    memory_value,
    memory_outgate,
    memory_ingate,
    memory_forget,
    forget_bias,
    forget_shift,
    stick_query,
    stick_key,
    stick_value,
    stick_bias,
    memory_gain,
    stick_gain,
    out_memory,
    out_stick,
):
    rows, half_feat = tokens.shape[1:]
    features = 2 * half_feat
    heads = forget_bias.shape[0]
    block, width = memory_query.shape
    dm = width // heads
    stick_width = stick_query.shape[1]
    ds = stick_width // heads
    lanes = 128
    n_out = 4
    half = rows // 2

    vmem = pl.BlockSpec(memory_space=pltpu.VMEM)
    smem = pl.BlockSpec(memory_space=pltpu.SMEM)
    anyw = pl.BlockSpec(memory_space=pl.ANY)
    dma = pltpu.SemaphoreType.DMA
    out = pl.pallas_call(
        functools.partial(kernel, n_sp, n_out),
        out_shape=pltpu.VMEM((half, features), bf16),
        in_specs=[vmem] * 4 + [smem, vmem, smem] + [vmem] * 2 + [anyw] * 9,
        out_specs=vmem,
        scratch_shapes=[
            pltpu.VMEM((rows, half_feat), bf16),
            pltpu.VMEM((rows, features), bf16),
            pltpu.VMEM((heads, 2, rows, block), bf16),
            pltpu.VMEM((4, block, width), bf16),
            pltpu.VMEM((4, heads, block, dm), bf16),
            pltpu.VMEM((3, features, stick_width), bf16),
            pltpu.VMEM((width + stick_width, features), bf16),
            pltpu.VMEM((4, heads, rows, dm), bf16),
            pltpu.VMEM((4, heads, rows, dm), bf16),
            pltpu.VMEM((4, heads, rows, dm), f32),
            pltpu.VMEM((4, heads, rows, dm), bf16),
            pltpu.VMEM((rows, stick_width), bf16),
            pltpu.VMEM((n_sp, 2, rows, stick_width), bf16),
            pltpu.VMEM((heads, rows, ds), f32),
            pltpu.VMEM((heads, rows, ds), f32),
            pltpu.VMEM((16, features), bf16),
            pltpu.VMEM((lanes, rows), f32),
            pltpu.VMEM((rows, lanes), f32),
            pltpu.VMEM((8, lanes), f32),
            pltpu.VMEM((heads, rows, lanes), f32),
            pltpu.VMEM((heads, dm, dm), f32),
            pltpu.VMEM((heads, dm, dm), bf16),
            pltpu.VMEM((heads, dm, dm), bf16),
            pltpu.VMEM((8, lanes), f32),
            pltpu.VMEM((8, lanes), f32),
            pltpu.VMEM((rows, width + stick_width), bf16),
            pltpu.VMEM((n_out, half, features // n_out), bf16),
            pltpu.VMEM((n_out, half, features // n_out), bf16),
            dma((9,)),
            dma((1,)),
            dma((1,)),
            dma((2 * heads,)),
            dma((2 * heads,)),
            dma((2 * heads,)),
            dma((2 * heads,)),
            dma((4 * heads,)),
            dma((4 * heads,)),
            dma((4 * heads,)),
            dma((4 * heads,)),
            dma((n_sp,)),
            dma((n_sp,)),
            dma((4 * heads,)),
            dma((4 * heads,)),
            dma((1,)),
            dma((1,)),
            dma((n_out,)),
            dma((n_out,)),
        ],
        compiler_params=pltpu.CompilerParams(
            collective_id=0, has_side_effects=True, vmem_limit_bytes=60 * 1024 * 1024
        ),
    )(
        tokens[0],
        norm_gain[None],
        memory_ingate.T,
        memory_forget.T,
        forget_bias,
        forget_shift[0].T,
        stick_bias,
        memory_gain[None],
        stick_gain[None],
        memory_key,
        memory_value,
        memory_query,
        memory_outgate,
        stick_query,
        stick_key,
        stick_value,
        out_memory,
        out_stick,
    )
    return out[None]


def solution(mesh):
    assert mesh.shape["fs"] == 4 and mesh.shape["tp"] == 2
    return jax.shard_map(
        functools.partial(per_device, mesh.shape["sp"]),
        mesh=mesh,
        in_specs=(
            P("fs", "sp", "tp"),
            P(),
            P("fs", "tp"),
            P("fs", "tp"),
            P("fs", "tp"),
            P("fs", "tp"),
            P(None, "tp"),
            P(None, "tp"),
            P("tp"),
            P("fs", "sp", "tp"),
            P(None, "tp"),
            P(None, "tp"),
            P(None, "tp"),
            P("tp"),
            P("tp"),
            P("tp"),
            P("tp", None),
            P("tp", None),
        ),
        out_specs=P("fs", ("sp", "tp"), None),
        check_vma=False,
    )
```

profile of v0, /device:TPU:17, one launch (start us, length us, event | category | flops | bytes accessed | tf_op | source)
XLA Modules:
  0.0 50.1 jit_solution(1671164609220082631)
XLA Ops:
  0.0 49.3 %shard_map.172 = bf16[128,2048]{1,0:T(8,128)(2,1)S(1)} custom-call(bf16[256,1024]{1,0:T(8,128)(2,1)} %bitcast.11, f32[1,2048]{1,0:T(1,128)} %bitcast.12, bf16[2,2048]{1,0:T(2,128)(2,1)} %bitcast.13, bf16[2,2048]{1,0:T(2,128)(2,1)} %bitcast.14, f32[2]{0:T(128)} %bias_ref.1, f32[2,256]{1,0:T(2,128)} %bitcast.15, f32[2]{0:T(128)} %sbias_ref.1, ...), custom_call_target="tpu_custom_call" | custom-call | tf_op jit(solution)/shard_map/pallas_call | solution.py:538
  49.3 0.8 %copy.20 = bf16[1,128,2048]{2,1,0:T(8,128)(2,1)} copy(bf16[1,128,2048]{2,1,0:T(8,128)(2,1)S(1)} %bitcast.10) | data formatting | bytes 1048576
where the time goes:
time: 50.3 us; the launch traced here: 50.1 us
  Pallas kernels  49.3 us (98%)
  local copies, waits for them, and re-layouts  0.8 us (2%)
    pallas_call x1, Pallas kernels, per_device(): pl.pallas_call(functools.partial(kernel, n_sp, n_out), out_shape=pltpu.VM...  49.3 us

commit v1 on v0

v1 whole, which is shorter than its diff:
```python
import functools

import jax
import jax.numpy as jnp
from jax import lax
from jax.experimental import pallas as pl
from jax.experimental.pallas import tpu as pltpu
from jax.sharding import PartitionSpec as P

MESH = pl.DeviceIdType.MESH
epsilon = 1e-06
floor_neg = -1e30
f32 = jnp.float32
bf16 = jnp.bfloat16

KEY, VALUE, QUERY, GATE = 0, 1, 2, 3


def dot(a, b, dims=((1,), (0,))):
    return lax.dot_general(a, b, (dims, ((), ())), preferred_element_type=f32)


def softplus(z):
    return jnp.maximum(z, 0.0) + jnp.log(1.0 + jnp.exp(-jnp.abs(z)))


def kernel(
    n_sp,
    n_out,
    tok_hbm,
    gain_hbm,
    ingate_hbm,
    forget_hbm,
    bias_ref,
    shift_hbm,
    sbias_ref,
    mgain_hbm,
    sgain_hbm,
    wk_hbm,
    wv_hbm,
    wq_hbm,
    wo_hbm,
    sq_hbm,
    sk_hbm,
    sv_hbm,
    om_hbm,
    os_hbm,
    out_ref,
    tok_ref,
    gain_ref,
    ingate_ref,
    forget_ref,
    shift_ref,
    mgain_ref,
    sgain_ref,
    tok_in,
    nrm,
    xg,
    wm,
    wg,
    ws,
    wout,
    sb,
    rb,
    own_part,
    proj,
    queries,
    kv,
    stick_acc,
    stick_run,
    far_out,
    far_in,
    gw,
    u_rows,
    u_cols,
    totals,
    tops,
    state_own,
    state_in,
    state_out,
    log_in,
    log_out,
    mix,
    early_out,
    ob,
    orb,
    load_sem,
    tok_s,
    tok_r,
    a2a_s,
    a2a_r,
    fwd_s,
    fwd_r,
    w_s,
    w_r,
    pass_s,
    z_r,
    rs_s,
    rs_r,
    kv_s,
    kv_r,
    far_s,
    far_r,
    chain_s,
    chain_r,
    log_s,
    log_r,
    out_s,
    out_r,
):
    f = lax.axis_index("fs")
    s = lax.axis_index("sp")
    t = lax.axis_index("tp")
    rows, half_feat = tok_ref.shape
    heads = state_own.shape[0]
    dm = state_own.shape[1]
    ds = sgain_ref.shape[1] // heads
    block = wm.shape[1]
    half = rows // 2
    other = 1 - t
    last = n_sp - 1
    helper = n_sp - 2

    def flip(bits):
        if bits == 1:
            return f + 1 - 2 * (f % 2)
        if bits == 2:
            return f + 2 - 4 * (f // 2)
        return 3 - f

    def remote(src, dst, send, recv, device):
        return pltpu.make_async_remote_copy(
            src_ref=src,
            dst_ref=dst,
            send_sem=send,
            recv_sem=recv,
            device_id=device,
            device_id_type=MESH,
        )

    barrier = pltpu.get_barrier_semaphore()
    pl.semaphore_signal(barrier, inc=1, device_id={"tp": other}, device_id_type=MESH)
    for bits in (1, 2):
        pl.semaphore_signal(barrier, inc=1, device_id={"fs": flip(bits)}, device_id_type=MESH)

    @pl.when(s > 0)
    def _():
        pl.semaphore_signal(barrier, inc=1, device_id={"sp": s - 1}, device_id_type=MESH)

    @pl.when(s < last)
    def _():
        pl.semaphore_signal(barrier, inc=1, device_id={"sp": s + 1}, device_id_type=MESH)

    def load(src, dst, at):
        return pltpu.make_async_copy(src, dst, load_sem.at[at])

    load(tok_hbm, tok_ref, 0).start()
    load(wk_hbm, wm.at[KEY], 1).start()
    load(wv_hbm, wm.at[VALUE], 1).start()
    load(gain_hbm, gain_ref, 2).start()
    load(sq_hbm, ws.at[0], 3).start()
    load(wq_hbm, wm.at[QUERY], 4).start()
    load(wo_hbm, wm.at[GATE], 4).start()
    load(sk_hbm, ws.at[1], 5).start()
    load(sv_hbm, ws.at[2], 5).start()
    load(ingate_hbm, ingate_ref, 6).start()
    load(forget_hbm, forget_ref, 7).start()
    load(shift_hbm, shift_ref, 8).start()
    load(om_hbm, wout.at[pl.ds(0, heads * dm)], 9).start()
    load(os_hbm, wout.at[pl.ds(heads * dm, heads * ds)], 9).start()
    load(mgain_hbm, mgain_ref, 10).start()
    load(sgain_hbm, sgain_ref, 11).start()

    def loaded(ref, at):
        pltpu.make_async_copy(ref, ref, load_sem.at[at]).wait()

    peers = 3 + jnp.where(s > 0, 1, 0) + jnp.where(s < last, 1, 0)
    pl.semaphore_wait(barrier, peers)

    loaded(tok_ref, 0)
    tok_copy = remote(tok_ref, tok_in, tok_s.at[0], tok_r.at[0], {"tp": other})
    tok_copy.start()

    def role(p, h):
        return (p + h) % 2

    def pair_bits(p, h):
        return 1 + role(p, h)

    def sum_bits(p, h):
        return 2 - role(p, h)

    first, second = [(KEY, 0), (VALUE, 0)], [(KEY, 1), (VALUE, 1)]
    third, fourth = [(QUERY, h) for h in range(heads)], [(GATE, h) for h in range(heads)]
    lines_p = block // 2
    parity = pl.ds(pl.multiple_of((s % 2) * lines_p, lines_p), lines_p)
    rest = pl.ds(pl.multiple_of((1 - s % 2) * lines_p, lines_p), lines_p)

    def stage(p, h):
        return h if p < 2 else p

    def weight_copy(p, h):
        return remote(
            wm.at[p, parity, pl.ds(h * dm, dm)], wg.at[p, h, parity], w_s.at[0],
            w_r.at[stage(p, h)], {"fs": flip(pair_bits(p, h))},
        )

    def rest_copy(p, h):
        return remote(
            wm.at[p, rest, pl.ds(h * dm, dm)], wg.at[p, h, rest], w_s.at[1],
            w_r.at[4], {"fs": flip(pair_bits(p, h))},
        )

    def pass_copy(p, h, at, to):
        return remote(
            wg.at[p, h, parity], wg.at[p, h, parity], pass_s.at[at], z_r.at[stage(p, h)], {"sp": to}
        )

    def both(p, h, lines):
        return wg.at[pl.ds(0, 2), h, lines] if p < 2 else wg.at[p, :, lines]

    def await_bytes(ref, sem):
        remote(ref, ref, pass_s.at[0], sem, {"tp": other}).wait_recv()

    def sent_bytes(ref, sem):
        remote(ref, ref, sem, z_r.at[0], {"tp": other}).wait_send()

    def send_weights(items):
        for p, h in items:
            weight_copy(p, h).start()

    def pass_weights(items):
        p, h = items[0]
        await_bytes(both(p, h, parity), w_r.at[stage(p, h)])
        for p, h in items:
            @pl.when(s > 0)
            def _():
                pass_copy(p, h, 0, s - 1).start()

            if p != GATE:
                @pl.when(s == helper)
                def _():
                    pass_copy(p, h, 1, s + 1).start()

    def rest_weights(items):
        p, h = items[0]
        if p != GATE:
            await_bytes(both(p, h, rest), z_r.at[stage(p, h)])
            return

        @pl.when(s < last)
        def _():
            await_bytes(both(p, h, rest), z_r.at[stage(p, h)])

        @pl.when(s == last)
        def _():
            await_bytes(both(p, h, rest), w_r.at[4])

    loaded(wm.at[pl.ds(KEY, 2)], 1)
    send_weights(first)
    send_weights(second)
    tok_copy.wait_recv()
    loaded(gain_ref, 2)

    step_rows = 32
    own_cols = pl.ds(pl.multiple_of(t * half_feat, half_feat), half_feat)
    far_cols = pl.ds(pl.multiple_of(other * half_feat, half_feat), half_feat)

    def norm_rows(i, _):
        at = pl.ds(pl.multiple_of(i * step_rows, step_rows), step_rows)
        own = tok_ref[at, :].astype(f32)
        far = tok_in[at, :].astype(f32)
        total = jnp.sum(own * own, axis=1, keepdims=True) + jnp.sum(far * far, axis=1, keepdims=True)
        scale = lax.rsqrt(total / (2 * half_feat) + epsilon)
        nrm[at, own_cols] = (own * scale * gain_ref[:, own_cols]).astype(bf16)
        nrm[at, far_cols] = (far * scale * gain_ref[:, far_cols]).astype(bf16)
        return 0

    lax.fori_loop(0, rows // step_rows, norm_rows, 0)

    my_rows = pl.ds(pl.multiple_of(t * half, half), half)

    def feature_block(index):
        return pl.ds(pl.multiple_of(index * block, block), block)

    a2a, fwd = {}, {}
    for r in range(2):
        for which in range(2):
            at = r * 2 + which
            to = flip(2 - r)
            a2a[at] = remote(
                nrm.at[my_rows, feature_block(to if which == 0 else flip(3))],
                xg.at[r, which, my_rows],
                a2a_s.at[0],
                a2a_r.at[at],
                {"fs": to},
            )
            a2a[at].start()
    loaded(wm.at[pl.ds(QUERY, 2)], 4)
    send_weights(third)
    send_weights(fourth)

    loaded(ws.at[0], 3)
    normed = nrm[...]
    queries[0] = dot(normed, ws[0]).astype(bf16)

    def query_copy():
        return remote(queries.at[0], queries.at[1], far_s.at[0], far_r.at[0], {"sp": s - 1})

    @pl.when(s == last)
    def _():
        query_copy().start()

    pass_weights(first)
    loaded(ws.at[pl.ds(1, 2)], 5)
    kv[0, 0] = dot(normed, ws[1]).astype(bf16)
    kv[0, 1] = dot(normed, ws[2]).astype(bf16)

    def kv_copy(d):
        return remote(kv.at[d - 1], kv.at[d], kv_s.at[d], kv_r.at[d], {"sp": s + 1})

    def kv_send(d):
        @pl.when((s < helper) & (s >= d - 1))
        def _():
            kv_copy(d).start()

    kv_send(1)

    row_at = lax.broadcasted_iota(jnp.int32, (rows, rows), 0)
    col_at = lax.broadcasted_iota(jnp.int32, (rows, rows), 1)
    loaded(ingate_ref, 6)
    loaded(forget_ref, 7)
    loaded(shift_ref, 8)
    gw[...] = jnp.zeros(gw.shape, bf16)
    gw[0:heads, :] = ingate_ref[...]
    gw[8 : 8 + heads, :] = forget_ref[...]
    gate = dot(gw[...], normed, ((1,), (1,)))
    triu = (row_at <= col_at).astype(f32)
    u_rows[...] = jnp.zeros(u_rows.shape, f32)
    for h in range(heads):
        log_forget = shift_ref[h : h + 1, :] - softplus(-(gate[8 + h : 9 + h, :] + bias_ref[h]))
        cumulative = lax.dot_general(
            jnp.broadcast_to(log_forget, (8, rows)), triu, (((1,), (0,)), ((), ())),
            precision=lax.Precision.HIGHEST, preferred_element_type=f32,
        )
        u_rows[h : h + 1, :] = gate[h : h + 1, :] - cumulative[0:1, :]
        totals[h : h + 1, :] = jnp.broadcast_to(
            cumulative[0:1, rows - 1 : rows], (1, totals.shape[1])
        )
    u_cols[...] = jnp.transpose(u_rows[...])
    pass_weights(second)

    def stick_part(at, h, kv_at, diagonal):
        cols = slice(h * ds, (h + 1) * ds)
        z = dot(queries[at, :, cols], kv[kv_at, 0, :, cols], ((1,), (1,)))
        z = z * ds ** (-0.5) + sbias_ref[h]
        keep = -softplus(z)
        visible = col_at < row_at
        if diagonal:
            kept = jnp.where(visible, keep, 0.0)
        else:
            kept = keep
        strict = (row_at > col_at).astype(bf16)
        high = kept.astype(bf16)
        low = (kept - high.astype(f32)).astype(bf16)
        after = dot(high, strict) + dot(low, strict)
        weights = jnp.exp(z + keep + after)
        if diagonal:
            weights = jnp.where(visible, weights, 0.0)
        part = dot(weights.astype(bf16), kv[kv_at, 1, :, cols])
        return part, jnp.sum(kept, axis=1, keepdims=True)

    def stick_first(at, diagonal):
        for h in range(heads):
            part, keep = stick_part(at, h, 0, diagonal)
            stick_acc[at, h] = part
            stick_run[at, h] = jnp.broadcast_to(keep, stick_run.shape[2:])

    def kv_forward(d):
        @pl.when((s >= d) & (s <= helper))
        def _():
            remote(kv.at[d - 1], kv.at[d], kv_s.at[d], kv_r.at[d], {"sp": s - 1}).wait_recv()

        @pl.when((s >= d) & (s < helper))
        def _():
            kv_copy(d + 1).start()

    def stick_span(d):
        @pl.when((s >= d) & (s <= helper))
        def _():
            def one(at, _):
                for h in range(heads):
                    part, keep = stick_part(at, h, d, False)
                    stick_acc[at, h] = stick_acc[at, h] + jnp.exp(stick_run[at, h]) * part
                    stick_run[at, h] = stick_run[at, h] + keep
                return 0

            lax.fori_loop(0, 1 + jnp.where(s == helper, 1, 0), one, 0)

    def over(low, high, step):
        if high > low:
            lax.fori_loop(low, high, lambda d, c: (step(d), c)[1], 0)

    stick_first(0, True)

    @pl.when(s == helper)
    def _():
        query_copy().wait_recv()
        stick_first(1, False)

    for at in (0, 2, 1, 3):
        a2a[at].wait_recv()
        r, which = divmod(at, 2)
        fwd[at] = remote(
            xg.at[r, which, my_rows],
            xg.at[r, which, my_rows],
            fwd_s.at[0],
            fwd_r.at[r],
            {"tp": other},
        )
        fwd[at].start()

    far_rows = pl.ds(pl.multiple_of(other * half, half), half)

    def rs_sem(p, h):
        return h if p < 2 else p + (h if p == GATE else 0)

    def rs_copy(p, h, lines):
        return remote(
            sb.at[p, h, lines], rb.at[p, h, lines], rs_s.at[0], rs_r.at[rs_sem(p, h)],
            {"fs": flip(sum_bits(p, h))},
        )

    def partials(items):
        rest_weights(items)
        for p, h in items:
            cols = slice(h * dm, (h + 1) * dm)
            r = role(p, h)
            sb[p, h] = (dot(xg[r, 0], wm[p, :, cols]) + dot(xg[r, 1], wg[p, h])).astype(bf16)
            rs_copy(p, h, pl.ds(0, rows)).start()

    def first_partials(items):
        rest_weights(items)
        for lines in (my_rows, far_rows):
            for p, h in items:
                cols = slice(h * dm, (h + 1) * dm)
                r = role(p, h)
                if lines is far_rows:
                    await_bytes(xg.at[r, :, far_rows], fwd_r.at[r])
                sb[p, h, lines] = (
                    dot(xg[r, 0, lines], wm[p, :, cols]) + dot(xg[r, 1, lines], wg[p, h])
                ).astype(bf16)
                rs_copy(p, h, lines).start()

    def own_partials(items):
        for p, h in items:
            cols = slice(h * dm, (h + 1) * dm)
            own_part[p, h] = dot(nrm[:, feature_block(f)], wm[p, :, cols]) + dot(
                nrm[:, feature_block(flip(pair_bits(p, h)))], wg[p, h]
            )

    def finish(p, h):
        return (own_part[p, h] + rb[p, h].astype(f32)).astype(bf16)

    def column(h):
        return u_cols[:, h : h + 1]

    def own_state(h):
        await_bytes(rb.at[pl.ds(0, 2), h], rs_r.at[h])
        proj[KEY, h] = (finish(KEY, h).astype(f32) * dm ** (-0.5)).astype(bf16)
        proj[VALUE, h] = finish(VALUE, h)
        u = column(h)
        top = jnp.max(u, axis=0, keepdims=True)
        weighted = (proj[KEY, h].astype(f32) * jnp.exp(u - top)).astype(bf16)
        state_own[h] = dot(weighted, proj[VALUE, h], ((0,), (0,)))

    def log_copy(h, to):
        return remote(log_out.at[h], log_in.at[h], log_s.at[0], log_r.at[h], {"sp": to})

    piece_dm = dm // 2
    pieces = 4

    def chain_copy(h, c, to):
        lines = pl.ds(c // 2 * piece_dm, piece_dm)
        cols = pl.ds(c % 2 * piece_dm, piece_dm)
        at = h * pieces + c
        return remote(
            state_out.at[h, lines, cols], state_in.at[h, lines, cols], chain_s.at[0], chain_r.at[at],
            {"sp": to},
        )

    def chain(h):
        @pl.when(s == 0)
        def _():
            log_in[h] = jnp.full(log_in.shape[1:], floor_neg, f32)
            state_in[h] = jnp.zeros(state_in.shape[1:], bf16)

        @pl.when(s > 0)
        def _():
            log_copy(h, s - 1).wait_recv()

        total = totals[h : h + 1, 0:1]
        early = total + log_in[h, 0:1, 0:1]
        late = total + jnp.max(column(h), axis=0, keepdims=True)
        top = jnp.maximum(early, late)

        @pl.when(s < last)
        def _():
            log_out[h] = jnp.broadcast_to(top, log_out.shape[1:])
            log_copy(h, s + 1).start()

        early, late = jnp.exp(early - top), jnp.exp(late - top)
        for c in range(pieces):
            lines = pl.ds(c // 2 * piece_dm, piece_dm)
            cols = pl.ds(c % 2 * piece_dm, piece_dm)

            @pl.when(s > 0)
            def _():
                chain_copy(h, c, s - 1).wait_recv()

            @pl.when(s < last)
            def _():
                state_out[h, lines, cols] = (
                    early * state_in[h, lines, cols].astype(f32) + late * state_own[h, lines, cols]
                ).astype(bf16)
                chain_copy(h, c, s + 1).start()

    def chain_if(where, h):
        @pl.when(where)
        def _():
            chain(h)

    pass_weights(third)
    over(1, min(2, n_sp - 1), kv_forward)
    first_partials(first)
    own_partials(first)
    partials(second)
    own_partials(second)
    pass_weights(fourth)

    @pl.when(s == last)
    def _():
        for p, h in fourth:
            rest_copy(p, h).start()

    over(1, min(2, n_sp - 1), stick_span)
    own_state(0)
    chain_if(s == 0, 0)
    over(2, n_sp - 1, kv_forward)
    over(2, n_sp - 1, stick_span)

    @pl.when(s == helper)
    def _():
        far_out[...] = stick_acc[1].astype(bf16)
        remote(far_out, far_in, far_s.at[1], far_r.at[1], {"sp": s + 1}).start()

    own_state(1)
    chain_if(s == 0, 1)
    chain_if(s == 1, 0)
    partials(third)
    own_partials(third)
    chain_if(s == 1, 1)
    chain_if(s == 2, 0)
    partials(fourth)
    own_partials(fourth)
    loaded(wout, 9)
    loaded(mgain_ref, 10)
    loaded(sgain_ref, 11)
    chain_if(s == 2, 1)

    causal = col_at <= row_at
    await_bytes(rb.at[QUERY], rs_r.at[QUERY])
    for h in range(heads):
        proj[QUERY, h] = finish(QUERY, h)
        masked = jnp.where(causal, u_rows[h : h + 1, :], floor_neg)
        top = jnp.max(masked, axis=1, keepdims=True)
        scores = dot(proj[QUERY, h], proj[KEY, h], ((1,), (1,))) * jnp.exp(masked - top)
        own_part[QUERY, h] = dot(scores.astype(bf16), proj[VALUE, h])
        tops[h] = jnp.broadcast_to(top, tops.shape[1:])

    @pl.when(s == last)
    def _():
        remote(far_out, far_in, far_s.at[1], far_r.at[1], {"sp": s - 1}).wait_recv()
        for h in range(heads):
            stick_acc[0, h] = stick_acc[0, h] + jnp.exp(stick_run[0, h]) * far_in[h].astype(f32)

    for h in range(heads):
        cols = slice(h * ds, (h + 1) * ds)
        out = stick_acc[0, h]
        scale = lax.rsqrt(jnp.mean(out * out, axis=1, keepdims=True) + epsilon)
        mix[:, heads * dm + h * ds : heads * dm + (h + 1) * ds] = (
            out * scale * sgain_ref[:, cols]
        ).astype(bf16)
    early_out[...] = dot(mix[:, heads * dm :], wout[heads * dm :, :])

    for h in range(heads):
        chain_if(s > 2, h)
        carried_max = log_in[h, 0:1, 0:1]
        top = tops[h, :, 0:1]
        running = jnp.maximum(carried_max, top)
        own_part[QUERY, h] = jnp.exp(top - running) * own_part[QUERY, h] + jnp.exp(
            carried_max - running
        ) * dot(proj[QUERY, h], state_in[h])
        await_bytes(rb.at[GATE, h], rs_r.at[GATE + h])
        gated = own_part[QUERY, h] / (1.0 + jnp.exp(-finish(GATE, h).astype(f32)))
        scale = lax.rsqrt(jnp.mean(gated * gated, axis=1, keepdims=True) + epsilon)
        cols = slice(h * dm, (h + 1) * dm)
        mix[:, cols] = (gated * scale * mgain_ref[:, cols]).astype(bf16)
        if h < heads - 1:
            early_out[...] = early_out[...] + dot(mix[:, cols], wout[cols, :])

    piece = wout.shape[1] // n_out
    lines = slice((heads - 1) * dm, heads * dm)
    copies = []
    for c in range(n_out):
        cols = slice(c * piece, (c + 1) * piece)
        ob[c] = (early_out[far_rows, cols] + dot(mix[far_rows, lines], wout[lines, cols])).astype(bf16)
        copy = remote(ob.at[c], orb.at[c], out_s.at[0], out_r.at[c], {"tp": other})
        copy.start()
        copies.append(copy)
    for c in range(n_out):
        cols = slice(c * piece, (c + 1) * piece)
        early_out[my_rows, cols] = early_out[my_rows, cols] + dot(mix[my_rows, lines], wout[lines, cols])
    for c in range(n_out):
        cols = slice(c * piece, (c + 1) * piece)
        copies[c].wait_recv()
        out_ref[:, cols] = (early_out[my_rows, cols] + orb[c].astype(f32)).astype(bf16)

    tok_copy.wait_send()
    sent_bytes(xg.at[:, :, my_rows], a2a_s.at[0])
    sent_bytes(xg.at[:, :, my_rows], fwd_s.at[0])
    sent_bytes(wm.at[:, parity], w_s.at[0])
    sent_bytes(sb, rs_s.at[0])
    sent_bytes(ob, out_s.at[0])

    @pl.when(s > 0)
    def _():
        sent_bytes(wg.at[:, :, parity], pass_s.at[0])

    @pl.when(s == helper)
    def _():
        sent_bytes(wg.at[pl.ds(0, 3), :, parity], pass_s.at[1])
        remote(far_out, far_in, far_s.at[1], far_r.at[1], {"sp": s + 1}).wait_send()

    @pl.when(s == last)
    def _():
        query_copy().wait_send()
        sent_bytes(wm.at[GATE, rest], w_s.at[1])

    @pl.when(s < last)
    def _():
        sent_bytes(log_out, log_s.at[0])
        sent_bytes(state_out, chain_s.at[0])

    def kv_done(d, c):
        @pl.when((s < helper) & (s >= d - 1))
        def _():
            kv_copy(d).wait_send()

        return c

    lax.fori_loop(1, n_sp - 1, kv_done, 0)


def per_device(
    n_sp,
    tokens,
    norm_gain,
    memory_query,
    memory_key,
    memory_value,
    memory_outgate,
    memory_ingate,
    memory_forget,
    forget_bias,
    forget_shift,
    stick_query,
    stick_key,
    stick_value,
    stick_bias,
    memory_gain,
    stick_gain,
    out_memory,
    out_stick,
):
    rows, half_feat = tokens.shape[1:]
    features = 2 * half_feat
    heads = forget_bias.shape[0]
    block, width = memory_query.shape
    dm = width // heads
    stick_width = stick_query.shape[1]
    ds = stick_width // heads
    lanes = 128
    n_out = 4
    half = rows // 2

    vmem = pl.BlockSpec(memory_space=pltpu.VMEM)
    smem = pl.BlockSpec(memory_space=pltpu.SMEM)
    anyw = pl.BlockSpec(memory_space=pl.ANY)
    dma = pltpu.SemaphoreType.DMA
    out = pl.pallas_call(
        functools.partial(kernel, n_sp, n_out),
        out_shape=pltpu.VMEM((half, features), bf16),
        in_specs=[anyw] * 4 + [smem, anyw, smem] + [anyw] * 11,
        out_specs=vmem,
        scratch_shapes=[
            pltpu.VMEM((rows, half_feat), bf16),
            pltpu.VMEM((1, features), f32),
            pltpu.VMEM((heads, features), bf16),
            pltpu.VMEM((heads, features), bf16),
            pltpu.VMEM((heads, rows), f32),
            pltpu.VMEM((1, width), f32),
            pltpu.VMEM((1, stick_width), f32),
            pltpu.VMEM((rows, half_feat), bf16),
            pltpu.VMEM((rows, features), bf16),
            pltpu.VMEM((2, 2, rows, block), bf16),
            pltpu.VMEM((4, block, width), bf16),
            pltpu.VMEM((4, heads, block, dm), bf16),
            pltpu.VMEM((3, features, stick_width), bf16),
            pltpu.VMEM((width + stick_width, features), bf16),
            pltpu.VMEM((4, heads, rows, dm), bf16),
            pltpu.VMEM((4, heads, rows, dm), bf16),
            pltpu.VMEM((4, heads, rows, dm), f32),
            pltpu.VMEM((4, heads, rows, dm), bf16),
            pltpu.VMEM((2, rows, stick_width), bf16),
            pltpu.VMEM((n_sp - 1, 2, rows, stick_width), bf16),
            pltpu.VMEM((2, heads, rows, ds), f32),
            pltpu.VMEM((2, heads, rows, ds), f32),
            pltpu.VMEM((heads, rows, ds), bf16),
            pltpu.VMEM((heads, rows, ds), bf16),
            pltpu.VMEM((16, features), bf16),
            pltpu.VMEM((lanes, rows), f32),
            pltpu.VMEM((rows, lanes), f32),
            pltpu.VMEM((8, lanes), f32),
            pltpu.VMEM((heads, rows, lanes), f32),
            pltpu.VMEM((heads, dm, dm), f32),
            pltpu.VMEM((heads, dm, dm), bf16),
            pltpu.VMEM((heads, dm, dm), bf16),
            pltpu.VMEM((heads, 8, lanes), f32),
            pltpu.VMEM((heads, 8, lanes), f32),
            pltpu.VMEM((rows, width + stick_width), bf16),
            pltpu.VMEM((rows, features), f32),
            pltpu.VMEM((n_out, half, features // n_out), bf16),
            pltpu.VMEM((n_out, half, features // n_out), bf16),
            dma((12,)),
            dma((1,)),
            dma((1,)),
            dma((1,)),
            dma((4,)),
            dma((1,)),
            dma((2,)),
            dma((2,)),
            dma((5,)),
            dma((2,)),
            dma((4,)),
            dma((1,)),
            dma((5,)),
            dma((n_sp - 1,)),
            dma((n_sp - 1,)),
            dma((2,)),
            dma((2,)),
            dma((1,)),
            dma((4 * heads,)),
            dma((1,)),
            dma((heads,)),
            dma((1,)),
            dma((n_out,)),
        ],
        compiler_params=pltpu.CompilerParams(
            collective_id=0, has_side_effects=True, vmem_limit_bytes=60 * 1024 * 1024
        ),
    )(
        tokens[0],
        norm_gain[None],
        memory_ingate.T,
        memory_forget.T,
        forget_bias,
        forget_shift[0].T,
        stick_bias,
        memory_gain[None],
        stick_gain[None],
        memory_key,
        memory_value,
        memory_query,
        memory_outgate,
        stick_query,
        stick_key,
        stick_value,
        out_memory,
        out_stick,
    )
    return out[None]


def solution(mesh):
    assert mesh.shape["fs"] == 4 and mesh.shape["tp"] == 2
    return jax.shard_map(
        functools.partial(per_device, mesh.shape["sp"]),
        mesh=mesh,
        in_specs=(
            P("fs", "sp", "tp"),
            P(),
            P("fs", "tp"),
            P("fs", "tp"),
            P("fs", "tp"),
            P("fs", "tp"),
            P(None, "tp"),
            P(None, "tp"),
            P("tp"),
            P("fs", "sp", "tp"),
            P(None, "tp"),
            P(None, "tp"),
            P(None, "tp"),
            P("tp"),
            P("tp"),
            P("tp"),
            P("tp", None),
            P("tp", None),
        ),
        out_specs=P("fs", ("sp", "tp"), None),
        check_vma=False,
    )
```

time: 50.3 us -> 43.7 us (0.87)
  Pallas kernels: 49.3 us -> 42.7 us
    pallas_call x1, Pallas kernels: 49.3 us -> 42.7 us  [per_device(): pl.pallas_call(functools.partial(kernel, n_sp, n_out), out_shape=pltpu.VM...]
where the time goes in v1:
time: 43.7 us; the launch traced here: 43.5 us
  Pallas kernels  42.7 us (98%)
  local copies, waits for them, and re-layouts  0.8 us (2%)
    pallas_call x1, Pallas kernels, per_device(): pl.pallas_call(functools.partial(kernel, n_sp, n_out), out_shape=pltpu.VM...  42.7 us

profile of v1, /device:TPU:17, one launch (start us, length us, event | category | flops | bytes accessed | tf_op | source)
XLA Modules:
  0.0 43.5 jit_solution(11294137054279073318)
XLA Ops:
  0.0 42.7 %shard_map.172 = bf16[128,2048]{1,0:T(8,128)(2,1)S(1)} custom-call(bf16[256,1024]{1,0:T(8,128)(2,1)} %bitcast.11, f32[1,2048]{1,0:T(1,128)} %bitcast.12, bf16[2,2048]{1,0:T(2,128)(2,1)} %bitcast.13, bf16[2,2048]{1,0:T(2,128)(2,1)} %bitcast.14, f32[2]{0:T(128)} %bias_ref.1, f32[2,256]{1,0:T(2,128)} %bitcast.15, f32[2]{0:T(128)} %sbias_ref.1, ...), custom_call_target="tpu_custom_call" | custom-call | tf_op jit(solution)/shard_map/pallas_call | solution.py:701
  42.7 0.8 %copy.20 = bf16[1,128,2048]{2,1,0:T(8,128)(2,1)} copy(bf16[1,128,2048]{2,1,0:T(8,128)(2,1)S(1)} %bitcast.10) | data formatting | bytes 1048576

commit v2 on v1

--- a/solution.py
+++ b/solution.py
@@ -31,9 +31,9 @@
     gain_hbm,
     ingate_hbm,
     forget_hbm,
-    bias_ref,
+    bias_hbm,
     shift_hbm,
-    sbias_ref,
+    sbias_hbm,
     mgain_hbm,
     sgain_hbm,
     wk_hbm,
@@ -51,6 +51,8 @@
     ingate_ref,
     forget_ref,
     shift_ref,
+    bias_ref,
+    sbias_ref,
     mgain_ref,
     sgain_ref,
     tok_in,
@@ -166,6 +168,8 @@
     load(ingate_hbm, ingate_ref, 6).start()
     load(forget_hbm, forget_ref, 7).start()
     load(shift_hbm, shift_ref, 8).start()
+    load(bias_hbm, bias_ref, 12).start()
+    load(sbias_hbm, sbias_ref, 13).start()
     load(om_hbm, wout.at[pl.ds(0, heads * dm)], 9).start()
     load(os_hbm, wout.at[pl.ds(heads * dm, heads * ds)], 9).start()
     load(mgain_hbm, mgain_ref, 10).start()
@@ -179,7 +183,6 @@
 
     loaded(tok_ref, 0)
     tok_copy = remote(tok_ref, tok_in, tok_s.at[0], tok_r.at[0], {"tp": other})
-    tok_copy.start()
 
     def role(p, h):
         return (p + h) % 2
@@ -192,28 +195,26 @@
 
     first, second = [(KEY, 0), (VALUE, 0)], [(KEY, 1), (VALUE, 1)]
     third, fourth = [(QUERY, h) for h in range(heads)], [(GATE, h) for h in range(heads)]
-    lines_p = block // 2
-    parity = pl.ds(pl.multiple_of((s % 2) * lines_p, lines_p), lines_p)
-    rest = pl.ds(pl.multiple_of((1 - s % 2) * lines_p, lines_p), lines_p)
+    def part(number, count, parts=1, offset=0):
+        size = block // count
+        return pl.ds(pl.multiple_of(number * size, size) + offset * (size // parts), size // parts)
+
+    parity, rest = part(s % 2, 2), part(1 - s % 2, 2)
+    splits = 4
+    fourth_own, fourth_rest, fourth_all = part(s % 2, 4), part(1 - s % 2, 4), part(1, 2)
 
     def stage(p, h):
         return h if p < 2 else p
 
-    def weight_copy(p, h):
+    def weight_copy(p, h, lines, at, sem):
         return remote(
-            wm.at[p, parity, pl.ds(h * dm, dm)], wg.at[p, h, parity], w_s.at[0],
-            w_r.at[stage(p, h)], {"fs": flip(pair_bits(p, h))},
+            wm.at[p, lines, pl.ds(h * dm, dm)], wg.at[p, h, lines], w_s.at[sem],
+            w_r.at[at], {"fs": flip(pair_bits(p, h))},
         )
 
-    def rest_copy(p, h):
+    def pass_copy(p, h, lines, at, to):
         return remote(
-            wm.at[p, rest, pl.ds(h * dm, dm)], wg.at[p, h, rest], w_s.at[1],
-            w_r.at[4], {"fs": flip(pair_bits(p, h))},
-        )
-
-    def pass_copy(p, h, at, to):
-        return remote(
-            wg.at[p, h, parity], wg.at[p, h, parity], pass_s.at[at], z_r.at[stage(p, h)], {"sp": to}
+            wg.at[p, h, lines], wg.at[p, h, lines], pass_s.at[at], z_r.at[stage(p, h)], {"sp": to}
         )
 
     def both(p, h, lines):
@@ -225,40 +226,52 @@
     def sent_bytes(ref, sem):
         remote(ref, ref, sem, z_r.at[0], {"tp": other}).wait_send()
 
-    def send_weights(items):
+    def send_weights(items, lines, at, sem=0):
         for p, h in items:
-            weight_copy(p, h).start()
-
-    def pass_weights(items):
+            weight_copy(p, h, lines, at, sem).start()
+
+    def pass_weights(items, lines, at, sem=0):
         p, h = items[0]
-        await_bytes(both(p, h, parity), w_r.at[stage(p, h)])
+        await_bytes(both(p, h, lines), w_r.at[at])
+        down = (s > 0) & (s < last) if items is fourth else s > 0
         for p, h in items:
-            @pl.when(s > 0)
+            @pl.when(down)
             def _():
-                pass_copy(p, h, 0, s - 1).start()
-
-            if p != GATE:
-                @pl.when(s == helper)
-                def _():
-                    pass_copy(p, h, 1, s + 1).start()
+                pass_copy(p, h, lines, sem, s - 1).start()
+
+            @pl.when(s == helper)
+            def _():
+                pass_copy(p, h, lines, 2 + sem, s + 1).start()
+
+    def first_lines(c):
+        return part(s % 2, 2, splits, c)
 
     def rest_weights(items):
         p, h = items[0]
-        if p != GATE:
+        if items is not fourth:
             await_bytes(both(p, h, rest), z_r.at[stage(p, h)])
             return
-
-        @pl.when(s < last)
-        def _():
-            await_bytes(both(p, h, rest), z_r.at[stage(p, h)])
-
-        @pl.when(s == last)
-        def _():
-            await_bytes(both(p, h, rest), w_r.at[4])
-
+        await_bytes(both(p, h, fourth_all), w_r.at[splits + 3])
+
+        @pl.when(s != helper)
+        def _():
+            await_bytes(both(p, h, fourth_rest), z_r.at[stage(p, h)])
+
+        @pl.when(s == helper)
+        def _():
+            await_bytes(both(p, h, fourth_rest), w_r.at[splits + 4])
+
+    def on_core(where, step):
+        @pl.when(t == where)
+        def _():
+            step()
+
+    on_core(1, tok_copy.start)
     loaded(wm.at[pl.ds(KEY, 2)], 1)
-    send_weights(first)
-    send_weights(second)
+    for c in range(splits):
+        send_weights(first, first_lines(c), c)
+    send_weights(second, parity, splits)
+    on_core(0, tok_copy.start)
     tok_copy.wait_recv()
     loaded(gain_ref, 2)
 
@@ -279,27 +292,38 @@
     lax.fori_loop(0, rows // step_rows, norm_rows, 0)
 
     my_rows = pl.ds(pl.multiple_of(t * half, half), half)
+    cut = rows * 7 // 16
+    core_rows = (pl.ds(0, cut), pl.ds(cut, rows - cut))
 
     def feature_block(index):
         return pl.ds(pl.multiple_of(index * block, block), block)
 
-    a2a, fwd = {}, {}
-    for r in range(2):
-        for which in range(2):
-            at = r * 2 + which
-            to = flip(2 - r)
-            a2a[at] = remote(
-                nrm.at[my_rows, feature_block(to if which == 0 else flip(3))],
-                xg.at[r, which, my_rows],
-                a2a_s.at[0],
-                a2a_r.at[at],
-                {"fs": to},
-            )
-            a2a[at].start()
+    def a2a_copy(core, r, which):
+        lines = core_rows[core]
+        to = flip(2 - r)
+        return remote(
+            nrm.at[lines, feature_block(to if which == 0 else flip(3))],
+            xg.at[r, which, lines],
+            a2a_s.at[0],
+            a2a_r.at[r * 2 + which],
+            {"fs": to},
+        )
+
+    def fwd_copy(core, r, which):
+        lines = core_rows[core]
+        return remote(
+            xg.at[r, which, lines], xg.at[r, which, lines], fwd_s.at[0], fwd_r.at[r], {"tp": other}
+        )
+
+    def a2a_start(core):
+        for r in range(2):
+            for which in range(2):
+                a2a_copy(core, r, which).start()
+
+    on_core(0, lambda: a2a_start(0))
+    on_core(1, lambda: a2a_start(1))
     loaded(wm.at[pl.ds(QUERY, 2)], 4)
-    send_weights(third)
-    send_weights(fourth)
-
+    on_core(0, lambda: send_weights(third, parity, splits + 1))
     loaded(ws.at[0], 3)
     normed = nrm[...]
     queries[0] = dot(normed, ws[0]).astype(bf16)
@@ -307,15 +331,6 @@
     def query_copy():
         return remote(queries.at[0], queries.at[1], far_s.at[0], far_r.at[0], {"sp": s - 1})
 
-    @pl.when(s == last)
-    def _():
-        query_copy().start()
-
-    pass_weights(first)
-    loaded(ws.at[pl.ds(1, 2)], 5)
-    kv[0, 0] = dot(normed, ws[1]).astype(bf16)
-    kv[0, 1] = dot(normed, ws[2]).astype(bf16)
-
     def kv_copy(d):
         return remote(kv.at[d - 1], kv.at[d], kv_s.at[d], kv_r.at[d], {"sp": s + 1})
 
@@ -324,13 +339,28 @@
         def _():
             kv_copy(d).start()
 
-    kv_send(1)
+    def kv_project():
+        loaded(ws.at[pl.ds(1, 2)], 5)
+        normed = nrm[...]
+        kv[0, 0] = dot(normed, ws[1]).astype(bf16)
+        kv[0, 1] = dot(normed, ws[2]).astype(bf16)
+        kv_send(1)
+
+    def pass_first():
+        for c in range(splits):
+            pass_weights(first, first_lines(c), c)
+
+    on_core(0, kv_project)
+    pass_first()
+    on_core(1, kv_project)
 
     row_at = lax.broadcasted_iota(jnp.int32, (rows, rows), 0)
     col_at = lax.broadcasted_iota(jnp.int32, (rows, rows), 1)
     loaded(ingate_ref, 6)
     loaded(forget_ref, 7)
     loaded(shift_ref, 8)
+    load(bias_hbm, bias_ref, 12).wait()
+    load(sbias_hbm, sbias_ref, 13).wait()
     gw[...] = jnp.zeros(gw.shape, bf16)
     gw[0:heads, :] = ingate_ref[...]
     gw[8 : 8 + heads, :] = forget_ref[...]
@@ -338,7 +368,7 @@
     triu = (row_at <= col_at).astype(f32)
     u_rows[...] = jnp.zeros(u_rows.shape, f32)
     for h in range(heads):
-        log_forget = shift_ref[h : h + 1, :] - softplus(-(gate[8 + h : 9 + h, :] + bias_ref[h]))
+        log_forget = shift_ref[h : h + 1, :] - softplus(-(gate[8 + h : 9 + h, :] + bias_ref[0:1, h : h + 1]))
         cumulative = lax.dot_general(
             jnp.broadcast_to(log_forget, (8, rows)), triu, (((1,), (0,)), ((), ())),
             precision=lax.Precision.HIGHEST, preferred_element_type=f32,
@@ -348,12 +378,18 @@
             cumulative[0:1, rows - 1 : rows], (1, totals.shape[1])
         )
     u_cols[...] = jnp.transpose(u_rows[...])
-    pass_weights(second)
+
+    pass_weights(second, parity, splits)
+
+    @pl.when(s == last)
+    def _():
+        query_copy().start()
+
 
     def stick_part(at, h, kv_at, diagonal):
         cols = slice(h * ds, (h + 1) * ds)
         z = dot(queries[at, :, cols], kv[kv_at, 0, :, cols], ((1,), (1,)))
-        z = z * ds ** (-0.5) + sbias_ref[h]
+        z = z * ds ** (-0.5) + sbias_ref[0:1, h : h + 1]
         keep = -softplus(z)
         visible = col_at < row_at
         if diagonal:
@@ -385,17 +421,21 @@
         def _():
             kv_copy(d + 1).start()
 
-    def stick_span(d):
+    def stick_span(at, d):
+        for h in range(heads):
+            part, keep = stick_part(at, h, d, False)
+            stick_acc[at, h] = stick_acc[at, h] + jnp.exp(stick_run[at, h]) * part
+            stick_run[at, h] = stick_run[at, h] + keep
+
+    def own_span(d):
         @pl.when((s >= d) & (s <= helper))
         def _():
-            def one(at, _):
-                for h in range(heads):
-                    part, keep = stick_part(at, h, d, False)
-                    stick_acc[at, h] = stick_acc[at, h] + jnp.exp(stick_run[at, h]) * part
-                    stick_run[at, h] = stick_run[at, h] + keep
-                return 0
-
-            lax.fori_loop(0, 1 + jnp.where(s == helper, 1, 0), one, 0)
+            stick_span(0, d)
+
+    def far_span(d):
+        @pl.when(s == helper)
+        def _():
+            stick_span(1, d)
 
     def over(low, high, step):
         if high > low:
@@ -403,23 +443,15 @@
 
     stick_first(0, True)
 
-    @pl.when(s == helper)
-    def _():
-        query_copy().wait_recv()
-        stick_first(1, False)
-
-    for at in (0, 2, 1, 3):
-        a2a[at].wait_recv()
-        r, which = divmod(at, 2)
-        fwd[at] = remote(
-            xg.at[r, which, my_rows],
-            xg.at[r, which, my_rows],
-            fwd_s.at[0],
-            fwd_r.at[r],
-            {"tp": other},
-        )
-        fwd[at].start()
-
+    def a2a_forward(core):
+        for which in range(2):
+            for r in range(2):
+                a2a_copy(core, r, which).wait_recv()
+                fwd_copy(core, r, which).start()
+
+    on_core(0, lambda: a2a_forward(0))
+    on_core(1, lambda: a2a_forward(1))
+    on_core(1, lambda: send_weights(third, parity, splits + 1))
     far_rows = pl.ds(pl.multiple_of(other * half, half), half)
 
     def rs_sem(p, h):
@@ -439,14 +471,14 @@
             sb[p, h] = (dot(xg[r, 0], wm[p, :, cols]) + dot(xg[r, 1], wg[p, h])).astype(bf16)
             rs_copy(p, h, pl.ds(0, rows)).start()
 
-    def first_partials(items):
-        rest_weights(items)
-        for lines in (my_rows, far_rows):
+    def first_partials(items, core):
+        for at in (core, 1 - core):
+            lines = core_rows[at]
             for p, h in items:
                 cols = slice(h * dm, (h + 1) * dm)
                 r = role(p, h)
-                if lines is far_rows:
-                    await_bytes(xg.at[r, :, far_rows], fwd_r.at[r])
+                if at != core:
+                    await_bytes(xg.at[r, :, lines], fwd_r.at[r])
                 sb[p, h, lines] = (
                     dot(xg[r, 0, lines], wm[p, :, cols]) + dot(xg[r, 1, lines], wg[p, h])
                 ).astype(bf16)
@@ -530,24 +562,34 @@
         def _():
             chain(h)
 
-    pass_weights(third)
     over(1, min(2, n_sp - 1), kv_forward)
-    first_partials(first)
+    rest_weights(first)
+    on_core(0, lambda: first_partials(first, 0))
+    on_core(1, lambda: first_partials(first, 1))
+    send_weights(fourth, fourth_own, splits + 2, 1)
     own_partials(first)
+    pass_weights(third, parity, splits + 1)
+    over(1, min(2, n_sp - 1), own_span)
     partials(second)
+    send_weights(fourth, fourth_all, splits + 3, 2)
+
+    @pl.when(s == helper)
+    def _():
+        send_weights(fourth, fourth_rest, splits + 4, 3)
+
     own_partials(second)
-    pass_weights(fourth)
-
-    @pl.when(s == last)
-    def _():
-        for p, h in fourth:
-            rest_copy(p, h).start()
-
-    over(1, min(2, n_sp - 1), stick_span)
     own_state(0)
     chain_if(s == 0, 0)
+    pass_weights(fourth, fourth_own, splits + 2, 1)
+    @pl.when(s == helper)
+    def _():
+        query_copy().wait_recv()
+        stick_first(1, False)
+
+    over(1, min(2, n_sp - 1), far_span)
     over(2, n_sp - 1, kv_forward)
-    over(2, n_sp - 1, stick_span)
+    over(2, n_sp - 1, own_span)
+    over(2, n_sp - 1, far_span)
 
     @pl.when(s == helper)
     def _():
@@ -558,10 +600,10 @@
     chain_if(s == 0, 1)
     chain_if(s == 1, 0)
     partials(third)
+    chain_if(s == 2, 0)
     own_partials(third)
+    partials(fourth)
     chain_if(s == 1, 1)
-    chain_if(s == 2, 0)
-    partials(fourth)
     own_partials(fourth)
     loaded(wout, 9)
     loaded(mgain_ref, 10)
@@ -627,25 +669,37 @@
         out_ref[:, cols] = (early_out[my_rows, cols] + orb[c].astype(f32)).astype(bf16)
 
     tok_copy.wait_send()
-    sent_bytes(xg.at[:, :, my_rows], a2a_s.at[0])
-    sent_bytes(xg.at[:, :, my_rows], fwd_s.at[0])
-    sent_bytes(wm.at[:, parity], w_s.at[0])
+
+    def a2a_sent(core):
+        sent_bytes(xg.at[:, :, core_rows[core]], a2a_s.at[0])
+        sent_bytes(xg.at[:, :, core_rows[core]], fwd_s.at[0])
+
+    on_core(0, lambda: a2a_sent(0))
+    on_core(1, lambda: a2a_sent(1))
+    sent_bytes(wm.at[pl.ds(0, 3), parity], w_s.at[0])
+    sent_bytes(wm.at[GATE, fourth_own], w_s.at[1])
+    sent_bytes(wm.at[GATE, fourth_all], w_s.at[2])
     sent_bytes(sb, rs_s.at[0])
     sent_bytes(ob, out_s.at[0])
 
     @pl.when(s > 0)
     def _():
-        sent_bytes(wg.at[:, :, parity], pass_s.at[0])
+        sent_bytes(wg.at[pl.ds(0, 3), :, parity], pass_s.at[0])
+
+    @pl.when((s > 0) & (s < last))
+    def _():
+        sent_bytes(wg.at[GATE, :, fourth_own], pass_s.at[1])
 
     @pl.when(s == helper)
     def _():
-        sent_bytes(wg.at[pl.ds(0, 3), :, parity], pass_s.at[1])
+        sent_bytes(wg.at[pl.ds(0, 3), :, parity], pass_s.at[2])
+        sent_bytes(wg.at[GATE, :, fourth_own], pass_s.at[3])
+        sent_bytes(wm.at[GATE, fourth_rest], w_s.at[3])
         remote(far_out, far_in, far_s.at[1], far_r.at[1], {"sp": s + 1}).wait_send()
 
     @pl.when(s == last)
     def _():
         query_copy().wait_send()
-        sent_bytes(wm.at[GATE, rest], w_s.at[1])
 
     @pl.when(s < last)
     def _():
@@ -695,13 +749,12 @@
     half = rows // 2
 
     vmem = pl.BlockSpec(memory_space=pltpu.VMEM)
-    smem = pl.BlockSpec(memory_space=pltpu.SMEM)
     anyw = pl.BlockSpec(memory_space=pl.ANY)
     dma = pltpu.SemaphoreType.DMA
     out = pl.pallas_call(
         functools.partial(kernel, n_sp, n_out),
         out_shape=pltpu.VMEM((half, features), bf16),
-        in_specs=[anyw] * 4 + [smem, anyw, smem] + [anyw] * 11,
+        in_specs=[anyw] * 18,
         out_specs=vmem,
         scratch_shapes=[
             pltpu.VMEM((rows, half_feat), bf16),
@@ -709,6 +762,8 @@
             pltpu.VMEM((heads, features), bf16),
             pltpu.VMEM((heads, features), bf16),
             pltpu.VMEM((heads, rows), f32),
+            pltpu.VMEM((1, heads), f32),
+            pltpu.VMEM((1, heads), f32),
             pltpu.VMEM((1, width), f32),
             pltpu.VMEM((1, stick_width), f32),
             pltpu.VMEM((rows, half_feat), bf16),
@@ -742,16 +797,16 @@
             pltpu.VMEM((rows, features), f32),
             pltpu.VMEM((n_out, half, features // n_out), bf16),
             pltpu.VMEM((n_out, half, features // n_out), bf16),
-            dma((12,)),
+            dma((14,)),
             dma((1,)),
             dma((1,)),
             dma((1,)),
             dma((4,)),
             dma((1,)),
             dma((2,)),
-            dma((2,)),
-            dma((5,)),
-            dma((2,)),
+            dma((4,)),
+            dma((9,)),
+            dma((4,)),
             dma((4,)),
             dma((1,)),
             dma((5,)),
@@ -774,9 +829,9 @@
         norm_gain[None],
         memory_ingate.T,
         memory_forget.T,
-        forget_bias,
+        forget_bias[None],
         forget_shift[0].T,
-        stick_bias,
+        stick_bias[None],
         memory_gain[None],
         stick_gain[None],
         memory_key,

time: 43.7 us -> 41 us (0.938)
  the two profiles are of different devices: /device:TPU:17 before, /device:TPU:25 now
where the time goes in v2:
time: 41 us; the launch traced here: 40.9 us
  Pallas kernels  40 us (98%)
  local copies, waits for them, and re-layouts  0.8 us (2%)
    pallas_call x1, Pallas kernels, per_device(): pl.pallas_call(functools.partial(kernel, n_sp, n_out), out_shape=pltpu.VM...  40 us

profile of v2, /device:TPU:25, one launch (start us, length us, event | category | flops | bytes accessed | tf_op | source)
XLA Modules:
  0.0 40.9 jit_solution(12467690317934895492)
XLA Ops:
  0.0 40.0 %shard_map.172 = bf16[128,2048]{1,0:T(8,128)(2,1)S(1)} custom-call(bf16[256,1024]{1,0:T(8,128)(2,1)} %bitcast.13, f32[1,2048]{1,0:T(1,128)} %bitcast.14, bf16[2,2048]{1,0:T(2,128)(2,1)} %bitcast.15, bf16[2,2048]{1,0:T(2,128)(2,1)} %bitcast.16, f32[1,2]{1,0:T(1,128)} %bitcast.20, f32[2,256]{1,0:T(2,128)} %bitcast.17, f32[1,2]{1,0:T(1,128)} %bitcast.21, ...), custom_call_target="tpu_custom_call" | custom-call | tf_op jit(solution)/shard_map/pallas_call | solution.py:754
  40.1 0.8 %copy.20 = bf16[1,128,2048]{2,1,0:T(8,128)(2,1)} copy(bf16[1,128,2048]{2,1,0:T(8,128)(2,1)S(1)} %bitcast.12) | data formatting | bytes 1048576

commit v3 on v2

--- a/solution.py
+++ b/solution.py
@@ -26,7 +26,6 @@
 
 def kernel(
     n_sp,
-    n_out,
     tok_hbm,
     gain_hbm,
     ingate_hbm,
@@ -48,13 +47,11 @@
     out_ref,
     tok_ref,
     gain_ref,
-    ingate_ref,
-    forget_ref,
+    gate_in,
     shift_ref,
     bias_ref,
     sbias_ref,
-    mgain_ref,
-    sgain_ref,
+    gains,
     tok_in,
     nrm,
     xg,
@@ -82,22 +79,18 @@
     state_out,
     log_in,
     log_out,
+    factors,
     mix,
+    mix_in,
+    wout_in,
     early_out,
-    ob,
-    orb,
     load_sem,
-    tok_s,
+    send_s,
     tok_r,
-    a2a_s,
     a2a_r,
-    fwd_s,
     fwd_r,
-    w_s,
     w_r,
-    pass_s,
     z_r,
-    rs_s,
     rs_r,
     kv_s,
     kv_r,
@@ -107,16 +100,16 @@
     chain_r,
     log_s,
     log_r,
-    out_s,
     out_r,
 ):
     f = lax.axis_index("fs")
     s = lax.axis_index("sp")
     t = lax.axis_index("tp")
     rows, half_feat = tok_ref.shape
+    features = wout.shape[1]
     heads = state_own.shape[0]
     dm = state_own.shape[1]
-    ds = sgain_ref.shape[1] // heads
+    ds = stick_acc.shape[3]
     block = wm.shape[1]
     half = rows // 2
     other = 1 - t
@@ -161,19 +154,19 @@
     load(wv_hbm, wm.at[VALUE], 1).start()
     load(gain_hbm, gain_ref, 2).start()
     load(sq_hbm, ws.at[0], 3).start()
+    load(sk_hbm, ws.at[1], 3).start()
+    load(sv_hbm, ws.at[2], 3).start()
     load(wq_hbm, wm.at[QUERY], 4).start()
     load(wo_hbm, wm.at[GATE], 4).start()
-    load(sk_hbm, ws.at[1], 5).start()
-    load(sv_hbm, ws.at[2], 5).start()
-    load(ingate_hbm, ingate_ref, 6).start()
-    load(forget_hbm, forget_ref, 7).start()
+    load(ingate_hbm, gate_in.at[0], 5).start()
+    load(forget_hbm, gate_in.at[1], 5).start()
     load(shift_hbm, shift_ref, 8).start()
-    load(bias_hbm, bias_ref, 12).start()
-    load(sbias_hbm, sbias_ref, 13).start()
+    load(bias_hbm, bias_ref, 6).start()
+    load(sbias_hbm, sbias_ref, 7).start()
     load(om_hbm, wout.at[pl.ds(0, heads * dm)], 9).start()
     load(os_hbm, wout.at[pl.ds(heads * dm, heads * ds)], 9).start()
-    load(mgain_hbm, mgain_ref, 10).start()
-    load(sgain_hbm, sgain_ref, 11).start()
+    load(mgain_hbm, gains.at[:, pl.ds(0, heads * dm)], 10).start()
+    load(sgain_hbm, gains.at[:, pl.ds(heads * dm, heads * ds)], 10).start()
 
     def loaded(ref, at):
         pltpu.make_async_copy(ref, ref, load_sem.at[at]).wait()
@@ -182,7 +175,7 @@
     pl.semaphore_wait(barrier, peers)
 
     loaded(tok_ref, 0)
-    tok_copy = remote(tok_ref, tok_in, tok_s.at[0], tok_r.at[0], {"tp": other})
+    tok_copy = remote(tok_ref, tok_in, send_s.at[2], tok_r.at[0], {"tp": other})
 
     def role(p, h):
         return (p + h) % 2
@@ -200,35 +193,35 @@
         return pl.ds(pl.multiple_of(number * size, size) + offset * (size // parts), size // parts)
 
     parity, rest = part(s % 2, 2), part(1 - s % 2, 2)
-    splits = 4
+    splits = 2
     fourth_own, fourth_rest, fourth_all = part(s % 2, 4), part(1 - s % 2, 4), part(1, 2)
 
     def stage(p, h):
         return h if p < 2 else p
 
-    def weight_copy(p, h, lines, at, sem):
+    def weight_copy(p, h, lines, at):
         return remote(
-            wm.at[p, lines, pl.ds(h * dm, dm)], wg.at[p, h, lines], w_s.at[sem],
+            wm.at[p, lines, pl.ds(h * dm, dm)], wg.at[p, h, lines], send_s.at[0],
             w_r.at[at], {"fs": flip(pair_bits(p, h))},
         )
 
     def pass_copy(p, h, lines, at, to):
         return remote(
-            wg.at[p, h, lines], wg.at[p, h, lines], pass_s.at[at], z_r.at[stage(p, h)], {"sp": to}
+            wg.at[p, h, lines], wg.at[p, h, lines], send_s.at[1], z_r.at[stage(p, h)], {"sp": to}
         )
 
     def both(p, h, lines):
         return wg.at[pl.ds(0, 2), h, lines] if p < 2 else wg.at[p, :, lines]
 
     def await_bytes(ref, sem):
-        remote(ref, ref, pass_s.at[0], sem, {"tp": other}).wait_recv()
+        remote(ref, ref, send_s.at[0], sem, {"tp": other}).wait_recv()
 
     def sent_bytes(ref, sem):
         remote(ref, ref, sem, z_r.at[0], {"tp": other}).wait_send()
 
-    def send_weights(items, lines, at, sem=0):
+    def send_weights(items, lines, at):
         for p, h in items:
-            weight_copy(p, h, lines, at, sem).start()
+            weight_copy(p, h, lines, at).start()
 
     def pass_weights(items, lines, at, sem=0):
         p, h = items[0]
@@ -239,6 +232,9 @@
             def _():
                 pass_copy(p, h, lines, sem, s - 1).start()
 
+            if items is fourth:
+                continue
+
             @pl.when(s == helper)
             def _():
                 pass_copy(p, h, lines, 2 + sem, s + 1).start()
@@ -251,15 +247,15 @@
         if items is not fourth:
             await_bytes(both(p, h, rest), z_r.at[stage(p, h)])
             return
-        await_bytes(both(p, h, fourth_all), w_r.at[splits + 3])
-
-        @pl.when(s != helper)
-        def _():
+
+        @pl.when(s < helper)
+        def _():
+            await_bytes(both(p, h, fourth_all), w_r.at[splits + 3])
             await_bytes(both(p, h, fourth_rest), z_r.at[stage(p, h)])
 
-        @pl.when(s == helper)
-        def _():
-            await_bytes(both(p, h, fourth_rest), w_r.at[splits + 4])
+        @pl.when(s >= helper)
+        def _():
+            await_bytes(both(p, h, pl.ds(0, block - block // 4)), w_r.at[splits + 3])
 
     def on_core(where, step):
         @pl.when(t == where)
@@ -304,15 +300,15 @@
         return remote(
             nrm.at[lines, feature_block(to if which == 0 else flip(3))],
             xg.at[r, which, lines],
-            a2a_s.at[0],
-            a2a_r.at[r * 2 + which],
+            send_s.at[0],
+            a2a_r.at[which],
             {"fs": to},
         )
 
     def fwd_copy(core, r, which):
         lines = core_rows[core]
         return remote(
-            xg.at[r, which, lines], xg.at[r, which, lines], fwd_s.at[0], fwd_r.at[r], {"tp": other}
+            xg.at[r, which, lines], xg.at[r, which, lines], send_s.at[0], fwd_r.at[0], {"tp": other}
         )
 
     def a2a_start(core):
@@ -323,8 +319,8 @@
     on_core(0, lambda: a2a_start(0))
     on_core(1, lambda: a2a_start(1))
     loaded(wm.at[pl.ds(QUERY, 2)], 4)
-    on_core(0, lambda: send_weights(third, parity, splits + 1))
-    loaded(ws.at[0], 3)
+    send_weights(third, parity, splits + 1)
+    loaded(ws, 3)
     normed = nrm[...]
     queries[0] = dot(normed, ws[0]).astype(bf16)
 
@@ -332,7 +328,7 @@
         return remote(queries.at[0], queries.at[1], far_s.at[0], far_r.at[0], {"sp": s - 1})
 
     def kv_copy(d):
-        return remote(kv.at[d - 1], kv.at[d], kv_s.at[d], kv_r.at[d], {"sp": s + 1})
+        return remote(kv.at[d - 1], kv.at[d], kv_s.at[d - 1], kv_r.at[d - 1], {"sp": s + 1})
 
     def kv_send(d):
         @pl.when((s < helper) & (s >= d - 1))
@@ -340,7 +336,6 @@
             kv_copy(d).start()
 
     def kv_project():
-        loaded(ws.at[pl.ds(1, 2)], 5)
         normed = nrm[...]
         kv[0, 0] = dot(normed, ws[1]).astype(bf16)
         kv[0, 1] = dot(normed, ws[2]).astype(bf16)
@@ -356,14 +351,13 @@
 
     row_at = lax.broadcasted_iota(jnp.int32, (rows, rows), 0)
     col_at = lax.broadcasted_iota(jnp.int32, (rows, rows), 1)
-    loaded(ingate_ref, 6)
-    loaded(forget_ref, 7)
+    loaded(gate_in, 5)
     loaded(shift_ref, 8)
-    load(bias_hbm, bias_ref, 12).wait()
-    load(sbias_hbm, sbias_ref, 13).wait()
+    load(bias_hbm, bias_ref, 6).wait()
+    load(sbias_hbm, sbias_ref, 7).wait()
     gw[...] = jnp.zeros(gw.shape, bf16)
-    gw[0:heads, :] = ingate_ref[...]
-    gw[8 : 8 + heads, :] = forget_ref[...]
+    gw[0:heads, :] = gate_in[0]
+    gw[8 : 8 + heads, :] = gate_in[1]
     gate = dot(gw[...], normed, ((1,), (1,)))
     triu = (row_at <= col_at).astype(f32)
     u_rows[...] = jnp.zeros(u_rows.shape, f32)
@@ -404,7 +398,7 @@
         if diagonal:
             weights = jnp.where(visible, weights, 0.0)
         part = dot(weights.astype(bf16), kv[kv_at, 1, :, cols])
-        return part, jnp.sum(kept, axis=1, keepdims=True)
+        return part, after[:, 0:1] + kept[:, 0:1]
 
     def stick_first(at, diagonal):
         for h in range(heads):
@@ -415,7 +409,7 @@
     def kv_forward(d):
         @pl.when((s >= d) & (s <= helper))
         def _():
-            remote(kv.at[d - 1], kv.at[d], kv_s.at[d], kv_r.at[d], {"sp": s - 1}).wait_recv()
+            remote(kv.at[d - 1], kv.at[d], kv_s.at[d - 1], kv_r.at[d - 1], {"sp": s - 1}).wait_recv()
 
         @pl.when((s >= d) & (s < helper))
         def _():
@@ -441,17 +435,19 @@
         if high > low:
             lax.fori_loop(low, high, lambda d, c: (step(d), c)[1], 0)
 
+    loaded(wout, 9)
+    wout_copy = remote(wout, wout_in, send_s.at[3], tok_r.at[1], {"tp": other})
+    wout_copy.start()
     stick_first(0, True)
 
     def a2a_forward(core):
         for which in range(2):
+            await_bytes(xg.at[:, which, core_rows[core]], a2a_r.at[which])
             for r in range(2):
-                a2a_copy(core, r, which).wait_recv()
                 fwd_copy(core, r, which).start()
 
     on_core(0, lambda: a2a_forward(0))
     on_core(1, lambda: a2a_forward(1))
-    on_core(1, lambda: send_weights(third, parity, splits + 1))
     far_rows = pl.ds(pl.multiple_of(other * half, half), half)
 
     def rs_sem(p, h):
@@ -459,7 +455,7 @@
 
     def rs_copy(p, h, lines):
         return remote(
-            sb.at[p, h, lines], rb.at[p, h, lines], rs_s.at[0], rs_r.at[rs_sem(p, h)],
+            sb.at[p, h, lines], rb.at[p, h, lines], send_s.at[1], rs_r.at[rs_sem(p, h)],
             {"fs": flip(sum_bits(p, h))},
         )
 
@@ -474,11 +470,11 @@
     def first_partials(items, core):
         for at in (core, 1 - core):
             lines = core_rows[at]
+            if at != core:
+                await_bytes(xg.at[:, :, lines], fwd_r.at[0])
             for p, h in items:
                 cols = slice(h * dm, (h + 1) * dm)
                 r = role(p, h)
-                if at != core:
-                    await_bytes(xg.at[r, :, lines], fwd_r.at[r])
                 sb[p, h, lines] = (
                     dot(xg[r, 0, lines], wm[p, :, cols]) + dot(xg[r, 1, lines], wg[p, h])
                 ).astype(bf16)
@@ -521,7 +517,7 @@
             {"sp": to},
         )
 
-    def chain(h):
+    def chain_logs(h):
         @pl.when(s == 0)
         def _():
             log_in[h] = jnp.full(log_in.shape[1:], floor_neg, f32)
@@ -541,8 +537,14 @@
             log_out[h] = jnp.broadcast_to(top, log_out.shape[1:])
             log_copy(h, s + 1).start()
 
-        early, late = jnp.exp(early - top), jnp.exp(late - top)
-        for c in range(pieces):
+        factors[h, 0] = jnp.broadcast_to(jnp.exp(early - top), factors.shape[2:])
+        factors[h, 1] = jnp.broadcast_to(jnp.exp(late - top), factors.shape[2:])
+
+    def chain(h, low=0, high=pieces):
+        if low == 0:
+            chain_logs(h)
+        early, late = factors[h, 0, 0:1, 0:1], factors[h, 1, 0:1, 0:1]
+        for c in range(low, high):
             lines = pl.ds(c // 2 * piece_dm, piece_dm)
             cols = pl.ds(c % 2 * piece_dm, piece_dm)
 
@@ -557,58 +559,106 @@
                 ).astype(bf16)
                 chain_copy(h, c, s + 1).start()
 
-    def chain_if(where, h):
+    def chain_if(where, h, low=0, high=pieces):
         @pl.when(where)
         def _():
-            chain(h)
+            chain(h, low, high)
 
     over(1, min(2, n_sp - 1), kv_forward)
     rest_weights(first)
     on_core(0, lambda: first_partials(first, 0))
     on_core(1, lambda: first_partials(first, 1))
-    send_weights(fourth, fourth_own, splits + 2, 1)
+
+    @pl.when(s > 0)
+    def _():
+        send_weights(fourth, fourth_own, splits + 2)
+
     own_partials(first)
     pass_weights(third, parity, splits + 1)
     over(1, min(2, n_sp - 1), own_span)
     partials(second)
-    send_weights(fourth, fourth_all, splits + 3, 2)
-
+    @pl.when(s == 0)
+    def _():
+        send_weights(fourth, fourth_own, splits + 2)
+
+    def send_fourth():
+        send_weights(fourth, fourth_all, splits + 3)
+
+        @pl.when(s >= helper)
+        def _():
+            send_weights(fourth, fourth_rest, splits + 3)
+
+    on_core(0, send_fourth)
+    own_partials(second)
     @pl.when(s == helper)
     def _():
-        send_weights(fourth, fourth_rest, splits + 4, 3)
-
-    own_partials(second)
+        query_copy().wait_recv()
+        stick_first(1, False)
+
+    over(1, min(2, n_sp - 1), far_span)
+
+    @pl.when(s == helper)
+    def _():
+        pass_weights(fourth, fourth_own, splits + 2, 1)
+
+    over(2, n_sp - 1, kv_forward)
+    over(2, n_sp - 1, far_span)
+
+    @pl.when(s == helper)
+    def _():
+        far_out[...] = stick_acc[1].astype(bf16)
+        remote(far_out, far_in, far_s.at[0], far_r.at[0], {"sp": s + 1}).start()
+
     own_state(0)
     chain_if(s == 0, 0)
-    pass_weights(fourth, fourth_own, splits + 2, 1)
-    @pl.when(s == helper)
-    def _():
-        query_copy().wait_recv()
-        stick_first(1, False)
-
-    over(1, min(2, n_sp - 1), far_span)
-    over(2, n_sp - 1, kv_forward)
-    over(2, n_sp - 1, own_span)
-    over(2, n_sp - 1, far_span)
-
-    @pl.when(s == helper)
-    def _():
-        far_out[...] = stick_acc[1].astype(bf16)
-        remote(far_out, far_in, far_s.at[1], far_r.at[1], {"sp": s + 1}).start()
-
+    on_core(1, send_fourth)
+
+    @pl.when((s > 0) & (s != helper))
+    def _():
+        pass_weights(fourth, fourth_own, splits + 2, 1)
+
+    chain_if(s == 1, 0)
     own_state(1)
     chain_if(s == 0, 1)
-    chain_if(s == 1, 0)
     partials(third)
     chain_if(s == 2, 0)
     own_partials(third)
+    chain_if(s == 1, 1)
+
+    @pl.when((s == 0) & (s != helper))
+    def _():
+        pass_weights(fourth, fourth_own, splits + 2, 1)
+
     partials(fourth)
-    chain_if(s == 1, 1)
     own_partials(fourth)
-    loaded(wout, 9)
-    loaded(mgain_ref, 10)
-    loaded(sgain_ref, 11)
-    chain_if(s == 2, 1)
+    loaded(gains, 10)
+    chain_if((s == 2) & (t == 1), 1)
+    over(2, n_sp - 1, own_span)
+    chain_if((s == 2) & (t == 0), 1, 0, 2)
+    width = heads * dm
+
+    def mix_copy(at, low, high):
+        return remote(
+            mix.at[far_rows, pl.ds(low, high - low)], mix_in.at[:, pl.ds(low, high - low)],
+            send_s.at[2], out_r.at[at], {"tp": other},
+        )
+
+    def stick_mix():
+        for h in range(heads):
+            cols = slice(h * ds, (h + 1) * ds)
+            out = stick_acc[0, h]
+            scale = lax.rsqrt(jnp.mean(out * out, axis=1, keepdims=True) + epsilon)
+            mix[:, heads * dm + h * ds : heads * dm + (h + 1) * ds] = (
+                out * scale * gains[:, heads * dm + h * ds : heads * dm + (h + 1) * ds]
+            ).astype(bf16)
+        mix_copy(heads, width, width + heads * ds).start()
+        early_out[...] = dot(mix[my_rows, width:], wout[width:, :])
+
+    @pl.when(s < last)
+    def _():
+        stick_mix()
+
+    chain_if((s == 2) & (t == 0), 1, 2, pieces)
 
     causal = col_at <= row_at
     await_bytes(rb.at[QUERY], rs_r.at[QUERY])
@@ -620,82 +670,70 @@
         own_part[QUERY, h] = dot(scores.astype(bf16), proj[VALUE, h])
         tops[h] = jnp.broadcast_to(top, tops.shape[1:])
 
+
     @pl.when(s == last)
     def _():
-        remote(far_out, far_in, far_s.at[1], far_r.at[1], {"sp": s - 1}).wait_recv()
+        remote(far_out, far_in, far_s.at[0], far_r.at[0], {"sp": s - 1}).wait_recv()
         for h in range(heads):
             stick_acc[0, h] = stick_acc[0, h] + jnp.exp(stick_run[0, h]) * far_in[h].astype(f32)
-
-    for h in range(heads):
-        cols = slice(h * ds, (h + 1) * ds)
-        out = stick_acc[0, h]
-        scale = lax.rsqrt(jnp.mean(out * out, axis=1, keepdims=True) + epsilon)
-        mix[:, heads * dm + h * ds : heads * dm + (h + 1) * ds] = (
-            out * scale * sgain_ref[:, cols]
-        ).astype(bf16)
-    early_out[...] = dot(mix[:, heads * dm :], wout[heads * dm :, :])
+        stick_mix()
+
+    wout_copy.wait_recv()
+
+    def mix_head(h, lines):
+        carried_max = log_in[h, 0:1, 0:1]
+        top = tops[h, lines, 0:1]
+        running = jnp.maximum(carried_max, top)
+        total = jnp.exp(top - running) * own_part[QUERY, h, lines] + jnp.exp(
+            carried_max - running
+        ) * dot(proj[QUERY, h, lines], state_in[h])
+        gate = (own_part[GATE, h, lines] + rb[GATE, h, lines].astype(f32)).astype(bf16)
+        gated = total / (1.0 + jnp.exp(-gate.astype(f32)))
+        scale = lax.rsqrt(jnp.mean(gated * gated, axis=1, keepdims=True) + epsilon)
+        cols = slice(h * dm, (h + 1) * dm)
+        mix[lines, cols] = (gated * scale * gains[:, cols]).astype(bf16)
 
     for h in range(heads):
         chain_if(s > 2, h)
-        carried_max = log_in[h, 0:1, 0:1]
-        top = tops[h, :, 0:1]
-        running = jnp.maximum(carried_max, top)
-        own_part[QUERY, h] = jnp.exp(top - running) * own_part[QUERY, h] + jnp.exp(
-            carried_max - running
-        ) * dot(proj[QUERY, h], state_in[h])
+        if h == 0:
+            mix_copy(heads, width, width + heads * ds).wait_recv()
+            early_out[...] = early_out[...] + dot(mix_in[:, width:], wout_in[width:, :])
         await_bytes(rb.at[GATE, h], rs_r.at[GATE + h])
-        gated = own_part[QUERY, h] / (1.0 + jnp.exp(-finish(GATE, h).astype(f32)))
-        scale = lax.rsqrt(jnp.mean(gated * gated, axis=1, keepdims=True) + epsilon)
+        mix_head(h, far_rows)
+        mix_copy(h, h * dm, (h + 1) * dm).start()
+        mix_head(h, my_rows)
+
+    early_out[...] = early_out[...] + dot(mix[my_rows, :width], wout[:width, :])
+    for h in range(heads):
         cols = slice(h * dm, (h + 1) * dm)
-        mix[:, cols] = (gated * scale * mgain_ref[:, cols]).astype(bf16)
+        mix_copy(h, h * dm, (h + 1) * dm).wait_recv()
+        total = early_out[...] + dot(mix_in[:, cols], wout_in[cols, :])
         if h < heads - 1:
-            early_out[...] = early_out[...] + dot(mix[:, cols], wout[cols, :])
-
-    piece = wout.shape[1] // n_out
-    lines = slice((heads - 1) * dm, heads * dm)
-    copies = []
-    for c in range(n_out):
-        cols = slice(c * piece, (c + 1) * piece)
-        ob[c] = (early_out[far_rows, cols] + dot(mix[far_rows, lines], wout[lines, cols])).astype(bf16)
-        copy = remote(ob.at[c], orb.at[c], out_s.at[0], out_r.at[c], {"tp": other})
-        copy.start()
-        copies.append(copy)
-    for c in range(n_out):
-        cols = slice(c * piece, (c + 1) * piece)
-        early_out[my_rows, cols] = early_out[my_rows, cols] + dot(mix[my_rows, lines], wout[lines, cols])
-    for c in range(n_out):
-        cols = slice(c * piece, (c + 1) * piece)
-        copies[c].wait_recv()
-        out_ref[:, cols] = (early_out[my_rows, cols] + orb[c].astype(f32)).astype(bf16)
-
-    tok_copy.wait_send()
-
-    def a2a_sent(core):
-        sent_bytes(xg.at[:, :, core_rows[core]], a2a_s.at[0])
-        sent_bytes(xg.at[:, :, core_rows[core]], fwd_s.at[0])
-
-    on_core(0, lambda: a2a_sent(0))
-    on_core(1, lambda: a2a_sent(1))
-    sent_bytes(wm.at[pl.ds(0, 3), parity], w_s.at[0])
-    sent_bytes(wm.at[GATE, fourth_own], w_s.at[1])
-    sent_bytes(wm.at[GATE, fourth_all], w_s.at[2])
-    sent_bytes(sb, rs_s.at[0])
-    sent_bytes(ob, out_s.at[0])
-
-    @pl.when(s > 0)
-    def _():
-        sent_bytes(wg.at[pl.ds(0, 3), :, parity], pass_s.at[0])
-
-    @pl.when((s > 0) & (s < last))
-    def _():
-        sent_bytes(wg.at[GATE, :, fourth_own], pass_s.at[1])
+            early_out[...] = total
+        else:
+            out_ref[...] = total.astype(bf16)
+
+    def sent_rows(where, count, sem):
+        @pl.when(where)
+        def _():
+            sent_bytes(wout.at[pl.ds(0, count)], sem)
+
+    quarter = block * width // (4 * features)
+    moved = [8 * lines * block // features for lines in (cut, rows - cut)]
+    for core in range(2):
+        sent_rows((t == core) & (s < helper), moved[core] + 9 * quarter, send_s.at[0])
+        sent_rows((t == core) & (s >= helper), moved[core] + 10 * quarter, send_s.at[0])
+    sums = 4 * rows * width // features
+    sent_rows(s == 0, sums, send_s.at[1])
+    sent_rows((s > 0) & (s < helper), sums + 7 * quarter, send_s.at[1])
+    sent_rows(s == helper, sums + 13 * quarter, send_s.at[1])
+    sent_rows(s == last, sums + 6 * quarter, send_s.at[1])
+    sent_bytes(wout.at[pl.ds(0, (rows * half_feat + half * wout.shape[0]) // features)], send_s.at[2])
+    wout_copy.wait_send()
 
     @pl.when(s == helper)
     def _():
-        sent_bytes(wg.at[pl.ds(0, 3), :, parity], pass_s.at[2])
-        sent_bytes(wg.at[GATE, :, fourth_own], pass_s.at[3])
-        sent_bytes(wm.at[GATE, fourth_rest], w_s.at[3])
-        remote(far_out, far_in, far_s.at[1], far_r.at[1], {"sp": s + 1}).wait_send()
+        remote(far_out, far_in, far_s.at[0], far_r.at[0], {"sp": s + 1}).wait_send()
 
     @pl.when(s == last)
     def _():
@@ -745,27 +783,24 @@
     stick_width = stick_query.shape[1]
     ds = stick_width // heads
     lanes = 128
-    n_out = 4
     half = rows // 2
 
     vmem = pl.BlockSpec(memory_space=pltpu.VMEM)
     anyw = pl.BlockSpec(memory_space=pl.ANY)
     dma = pltpu.SemaphoreType.DMA
     out = pl.pallas_call(
-        functools.partial(kernel, n_sp, n_out),
+        functools.partial(kernel, n_sp),
         out_shape=pltpu.VMEM((half, features), bf16),
         in_specs=[anyw] * 18,
         out_specs=vmem,
         scratch_shapes=[
             pltpu.VMEM((rows, half_feat), bf16),
             pltpu.VMEM((1, features), f32),
-            pltpu.VMEM((heads, features), bf16),
-            pltpu.VMEM((heads, features), bf16),
+            pltpu.VMEM((2, heads, features), bf16),
             pltpu.VMEM((heads, rows), f32),
             pltpu.VMEM((1, heads), f32),
             pltpu.VMEM((1, heads), f32),
-            pltpu.VMEM((1, width), f32),
-            pltpu.VMEM((1, stick_width), f32),
+            pltpu.VMEM((1, width + stick_width), f32),
             pltpu.VMEM((rows, half_feat), bf16),
             pltpu.VMEM((rows, features), bf16),
             pltpu.VMEM((2, 2, rows, block), bf16),
@@ -793,33 +828,28 @@
             pltpu.VMEM((heads, dm, dm), bf16),
             pltpu.VMEM((heads, 8, lanes), f32),
             pltpu.VMEM((heads, 8, lanes), f32),
+            pltpu.VMEM((heads, 2, 8, lanes), f32),
             pltpu.VMEM((rows, width + stick_width), bf16),
-            pltpu.VMEM((rows, features), f32),
-            pltpu.VMEM((n_out, half, features // n_out), bf16),
-            pltpu.VMEM((n_out, half, features // n_out), bf16),
-            dma((14,)),
+            pltpu.VMEM((half, width + stick_width), bf16),
+            pltpu.VMEM((width + stick_width, features), bf16),
+            pltpu.VMEM((half, features), f32),
+            dma((11,)),
+            dma((4,)),
+            dma((2,)),
+            dma((2,)),
+            dma((1,)),
+            dma((6,)),
+            dma((4,)),
+            dma((5,)),
+            dma((n_sp - 2,)),
+            dma((n_sp - 2,)),
             dma((1,)),
             dma((1,)),
-            dma((1,)),
-            dma((4,)),
-            dma((1,)),
-            dma((2,)),
-            dma((4,)),
-            dma((9,)),
-            dma((4,)),
-            dma((4,)),
-            dma((1,)),
-            dma((5,)),
-            dma((n_sp - 1,)),
-            dma((n_sp - 1,)),
-            dma((2,)),
-            dma((2,)),
             dma((1,)),
             dma((4 * heads,)),
             dma((1,)),
             dma((heads,)),
-            dma((1,)),
-            dma((n_out,)),
+            dma((heads + 1,)),
         ],
         compiler_params=pltpu.CompilerParams(
             collective_id=0, has_side_effects=True, vmem_limit_bytes=60 * 1024 * 1024

time: 41 us -> 39.5 us (0.963)
  the two profiles are of different devices: /device:TPU:25 before, /device:TPU:17 now
where the time goes in v3:
time: 39.5 us; the launch traced here: 39 us
  Pallas kernels  38.2 us (97%)
  local copies, waits for them, and re-layouts  0.8 us (2%)
    pallas_call x1, Pallas kernels, per_device(): pl.pallas_call(functools.partial(kernel, n_sp), out_shape=pltpu.VMEM((hal...  38.2 us
    unnamed x1, local copies, waits for them, and re-layouts  0.8 us

profile of v3, /device:TPU:17, one launch (start us, length us, event | category | flops | bytes accessed | tf_op | source)
XLA Modules:
  0.0 39.0 jit_solution(3225560983591900082)
XLA Ops:
  0.0 38.2 %shard_map.172 = bf16[128,2048]{1,0:T(8,128)(2,1)S(1)} custom-call(bf16[256,1024]{1,0:T(8,128)(2,1)} %bitcast.13, f32[1,2048]{1,0:T(1,128)} %bitcast.14, bf16[2,2048]{1,0:T(2,128)(2,1)} %bitcast.15, bf16[2,2048]{1,0:T(2,128)(2,1)} %bitcast.16, f32[1,2]{1,0:T(1,128)} %bitcast.20, f32[2,256]{1,0:T(2,128)} %bitcast.17, f32[1,2]{1,0:T(1,128)} %bitcast.21, ...), custom_call_target="tpu_custom_call" | custom-call | tf_op jit(solution)/shard_map/pallas_call | solution.py:791
  38.2 0.8 %copy.20 = bf16[1,128,2048]{2,1,0:T(8,128)(2,1)} copy(bf16[1,128,2048]{2,1,0:T(8,128)(2,1)S(1)} %bitcast.12) | data formatting | bytes 1048576

commit v4 on v3

--- a/solution.py
+++ b/solution.py
@@ -568,19 +568,11 @@
     rest_weights(first)
     on_core(0, lambda: first_partials(first, 0))
     on_core(1, lambda: first_partials(first, 1))
-
-    @pl.when(s > 0)
-    def _():
-        send_weights(fourth, fourth_own, splits + 2)
-
+    send_weights(fourth, fourth_own, splits + 2)
     own_partials(first)
     pass_weights(third, parity, splits + 1)
     over(1, min(2, n_sp - 1), own_span)
     partials(second)
-    @pl.when(s == 0)
-    def _():
-        send_weights(fourth, fourth_own, splits + 2)
-
     def send_fourth():
         send_weights(fourth, fourth_all, splits + 3)
 
@@ -588,7 +580,7 @@
         def _():
             send_weights(fourth, fourth_rest, splits + 3)
 
-    on_core(0, send_fourth)
+    send_fourth()
     own_partials(second)
     @pl.when(s == helper)
     def _():
@@ -611,23 +603,26 @@
 
     own_state(0)
     chain_if(s == 0, 0)
-    on_core(1, send_fourth)
-
-    @pl.when((s > 0) & (s != helper))
+
+    @pl.when((s > 0) & (s < helper) & (t == 0))
     def _():
         pass_weights(fourth, fourth_own, splits + 2, 1)
 
     chain_if(s == 1, 0)
     own_state(1)
     chain_if(s == 0, 1)
+    @pl.when((s > 0) & (s < helper) & (t == 1))
+    def _():
+        pass_weights(fourth, fourth_own, splits + 2, 1)
+
     partials(third)
     chain_if(s == 2, 0)
     own_partials(third)
     chain_if(s == 1, 1)
 
-    @pl.when((s == 0) & (s != helper))
-    def _():
-        pass_weights(fourth, fourth_own, splits + 2, 1)
+    @pl.when((s == 0) | (s == last))
+    def _():
+        await_bytes(both(GATE, 0, fourth_own), w_r.at[splits + 2])
 
     partials(fourth)
     own_partials(fourth)

time: 39.5 us -> 39.1 us (0.990)
  no operation moved by 1% of the time
where the time goes in v4:
time: 39.1 us; the launch traced here: 38.7 us
  Pallas kernels  37.9 us (97%)
  local copies, waits for them, and re-layouts  0.8 us (2%)
    pallas_call x1, Pallas kernels, per_device(): pl.pallas_call(functools.partial(kernel, n_sp), out_shape=pltpu.VMEM((hal...  37.9 us
    unnamed x1, local copies, waits for them, and re-layouts  0.8 us

profile of v4, /device:TPU:17, one launch (start us, length us, event | category | flops | bytes accessed | tf_op | source)
XLA Modules:
  0.0 38.7 jit_solution(4262390088516929403)
XLA Ops:
  0.0 37.9 %shard_map.172 = bf16[128,2048]{1,0:T(8,128)(2,1)S(1)} custom-call(bf16[256,1024]{1,0:T(8,128)(2,1)} %bitcast.13, f32[1,2048]{1,0:T(1,128)} %bitcast.14, bf16[2,2048]{1,0:T(2,128)(2,1)} %bitcast.15, bf16[2,2048]{1,0:T(2,128)(2,1)} %bitcast.16, f32[1,2]{1,0:T(1,128)} %bitcast.20, f32[2,256]{1,0:T(2,128)} %bitcast.17, f32[1,2]{1,0:T(1,128)} %bitcast.21, ...), custom_call_target="tpu_custom_call" | custom-call | tf_op jit(solution)/shard_map/pallas_call | solution.py:786
  37.9 0.8 %copy.20 = bf16[1,128,2048]{2,1,0:T(8,128)(2,1)} copy(bf16[1,128,2048]{2,1,0:T(8,128)(2,1)S(1)} %bitcast.12) | data formatting | bytes 1048576

commit v5 on v4

--- a/solution.py
+++ b/solution.py
@@ -696,6 +696,7 @@
         await_bytes(rb.at[GATE, h], rs_r.at[GATE + h])
         mix_head(h, far_rows)
         mix_copy(h, h * dm, (h + 1) * dm).start()
+    for h in range(heads):
         mix_head(h, my_rows)
 
     early_out[...] = early_out[...] + dot(mix[my_rows, :width], wout[:width, :])

time: 39.1 us -> 39 us (level)
  no operation moved by 1% of the time
where the time goes in v5:
time: 39 us; the launch traced here: 38.5 us
  Pallas kernels  37.7 us (97%)
  local copies, waits for them, and re-layouts  0.8 us (2%)
    pallas_call x1, Pallas kernels, per_device(): pl.pallas_call(functools.partial(kernel, n_sp), out_shape=pltpu.VMEM((hal...  37.7 us
    unnamed x1, local copies, waits for them, and re-layouts  0.8 us

profile of v5, /device:TPU:17, one launch (start us, length us, event | category | flops | bytes accessed | tf_op | source)
XLA Modules:
  0.0 38.5 jit_solution(5466667271619139092)
XLA Ops:
  0.0 37.7 %shard_map.172 = bf16[128,2048]{1,0:T(8,128)(2,1)S(1)} custom-call(bf16[256,1024]{1,0:T(8,128)(2,1)} %bitcast.13, f32[1,2048]{1,0:T(1,128)} %bitcast.14, bf16[2,2048]{1,0:T(2,128)(2,1)} %bitcast.15, bf16[2,2048]{1,0:T(2,128)(2,1)} %bitcast.16, f32[1,2]{1,0:T(1,128)} %bitcast.20, f32[2,256]{1,0:T(2,128)} %bitcast.17, f32[1,2]{1,0:T(1,128)} %bitcast.21, ...), custom_call_target="tpu_custom_call" | custom-call | tf_op jit(solution)/shard_map/pallas_call | solution.py:787
  37.7 0.8 %copy.20 = bf16[1,128,2048]{2,1,0:T(8,128)(2,1)} copy(bf16[1,128,2048]{2,1,0:T(8,128)(2,1)S(1)} %bitcast.12) | data formatting | bytes 1048576
